TPU v7x, 32 devices: a whole 2x2x4 slice. The times are simulated.
32 devices in a mesh: fs: 8 (over z, y), tp: 4 (over x, core).
Axes of the slice: x: 2, y: 2, z: 4, core: 2. Of those that a mesh axis runs over, the one named last changes fastest.
Arguments:
- tokens: bfloat16 [4096, 2048], P('fs'), may hold values from -6 to 6
- norm_gain: float32 [2048], P('fs'), may hold values from 0.1 to 1.9
- gate_weight: float32 [2048, 6144], P('fs', 'tp'), may hold values from -0.125 to 0.125
- up_weight: float32 [2048, 6144], P('fs', 'tp'), may hold values from -0.125 to 0.125
- down_weight: float32 [6144, 2048], P('fs', 'tp'), may hold values from -0.109375 to 0.109375
Outputs:
- mixed: bfloat16 [4096, 2048], P('fs', 'tp')
- gate_out: bfloat16 [2048, 6144], P(None, 'tp')
- up_out: bfloat16 [2048, 6144], P(None, 'tp')
- down_out: bfloat16 [6144, 2048], P('tp')
All inputs are finite; a program needn't handle non-finite values.
Results may differ from a plain program's by a relative error of at most 0.014.
Values may be sent and summed in bfloat16 or wider, within the bound.
A program may use at most 128 MiB of HBM per device.

v0:
```python
import functools

import jax
import jax.numpy as jnp
from jax import lax
from jax.experimental import pallas as pl
from jax.experimental.pallas import tpu as pltpu
from jax.sharding import PartitionSpec as P

MESH = pl.DeviceIdType.MESH
GRANT = 16 * 1024 * 1024


def lines(fs):
    y = 1
    while 2 * (2 * y) * (2 * y) <= fs:
        y *= 2
    return fs // y, y


def gather_kernel(
    Z, Y, T, nk, nd, detour,
    g_ref, u_ref, d_ref, x_ref, wg, wu, wd, hidden,
    normed, s_up, s_dn, s_y, r_w, s_det, d_up, d_dn, d_y, r_d, s_one, r_one,
):
    f, t = lax.axis_index("fs"), lax.axis_index("tp")
    z, y = f // Y, lax.rem(f, Y)
    has_up, has_dn = z < Z - 1, z > 0
    up, dn = (f + Y, t), (f - Y, t)
    others = [lax.rem(y + i, Y) for i in range(1, Y)]
    across = [(z * Y + o, t) for o in others]
    rows = g_ref.shape[0]
    ck = rows // nk
    rows_d, cols_d = d_ref.shape
    cd = rows_d // nd
    own, full = (g_ref, u_ref), (wg, wu)

    def when(cond, fn):
        pl.when(cond)(fn)

    barrier = pltpu.get_barrier_semaphore()

    def greet(dev):
        pl.semaphore_signal(barrier, inc=1, device_id=dev, device_id_type=MESH)

    when(has_up, lambda: greet(up))
    when(has_dn, lambda: greet(dn))
    for dev in across:
        greet(dev)
    for i in range(1, T):
        greet((f, lax.rem(t + i, T)))
    pl.semaphore_wait(barrier, Y + T - 2 + has_up.astype(jnp.int32) + has_dn.astype(jnp.int32))

    def copy(src, dst, ss, rs, dev):
        return pltpu.make_async_remote_copy(
            src_ref=src, dst_ref=dst, send_sem=ss, recv_sem=rs, device_id=dev, device_id_type=MESH
        )

    def part(a, source, k):
        return full[a].at[pl.ds(pl.multiple_of(source * rows + k * ck, ck), ck), :]

    def weight(a, k, source, ss, dev, mine=False):
        src = own[a].at[pl.ds(k * ck, ck), :] if mine else part(a, source, k)
        return copy(src, part(a, source, k), ss, r_w.at[source, a, k], dev)

    def arrived(a, k, source):
        weight(a, k, source, s_det.at[0, a, k], (f, lax.rem(t + 1, T))).wait_recv()

    pieces = [(k, a) for k in range(nk) for a in range(2)]
    sent = []

    def start(cond, make):
        sent.append((cond, make))
        if cond is None:
            make().start()
        else:
            when(cond, lambda: make().start())

    for k, a in pieces:
        start(has_up, lambda k=k, a=a: weight(a, k, f, s_up.at[z, a, k], up, True))
        start(has_dn, lambda k=k, a=a: weight(a, k, f, s_dn.at[z, a, k], dn, True))
        for i in range(Y - 1):
            start(None, lambda k=k, a=a, i=i: weight(a, k, f, s_y.at[i, z, a, k], across[i], True))

    def column(owner):
        return wd.at[
            pl.ds(pl.multiple_of(y * rows_d, rows_d), rows_d),
            pl.ds(pl.multiple_of(owner * cols_d, cols_d), cols_d),
        ]

    def first(owner, dev):
        return copy(d_ref, column(owner), s_one.at[0], r_one.at[owner], dev)

    start(z != t, lambda: first(t, (f, z)))

    for a in range(2):
        full[a][pl.ds(pl.multiple_of(f * rows, rows), rows), :] = own[a][...]

    def keep():
        wd[
            pl.ds(pl.multiple_of(y * rows_d, rows_d), rows_d),
            pl.ds(pl.multiple_of(t * cols_d, cols_d), cols_d),
        ] = d_ref[...]

    when(z == t, keep)

    n = x_ref.shape[0]
    slab = 64 if n % 64 == 0 else n

    @pl.loop(0, n // slab)
    def _(i):
        at = pl.ds(pl.multiple_of(i * slab, slab), slab)
        v = x_ref[at, :].astype(jnp.float32)
        normed[at, :] = (v * lax.rsqrt(jnp.mean(v * v, axis=1, keepdims=True) + 1e-05)).astype(jnp.bfloat16)

    for k, a in pieces:
        if k >= detour:
            continue
        source = across[0][0]
        arrived(a, k, source)
        start(has_up, lambda k=k, a=a, s=source: weight(a, k, s, s_det.at[0, a, k], up))
        start(has_dn, lambda k=k, a=a, s=source: weight(a, k, s, s_det.at[1, a, k], dn))

    for step in range(1, Z):
        for k, a in pieces:
            for sign in (-1, 1):
                zs = z + sign * step
                source = zs * Y + y
                valid = zs >= 0 if sign < 0 else zs < Z
                onward = jnp.logical_and(valid, has_up if sign < 0 else has_dn)
                when(valid, lambda a=a, k=k, s=source: arrived(a, k, s))
                if sign < 0:
                    start(onward, lambda a=a, k=k, s=source, q=zs: weight(a, k, s, s_up.at[q, a, k], up))
                else:
                    start(onward, lambda a=a, k=k, s=source, q=zs: weight(a, k, s, s_dn.at[q, a, k], dn))
                if step == 1 and k < detour:
                    continue
                for i in range(Y - 1):
                    start(valid, lambda a=a, k=k, s=source, q=zs, i=i: weight(a, k, s, s_y.at[i, q, a, k], across[i]))

    def rows_of(line, k):
        return wd.at[pl.ds(pl.multiple_of(line * rows_d + k * cd, cd), cd), :]

    def down(k, ss, dev, line):
        return copy(rows_of(line, k), rows_of(line, k), ss, r_d.at[line, k], dev)

    def down_arrived(k, line):
        down(k, d_up.at[k], (f, lax.rem(t + 1, T)), line).wait_recv()

    def assemble():
        for i in range(1, T):
            owner = lax.rem(t + i, T)
            first(owner, (f, owner)).wait_recv()

    when(z == t, assemble)
    go_up = jnp.logical_and(z >= t, has_up)
    go_dn = jnp.logical_and(z <= t, has_dn)
    for k in range(nd):
        when(z != t, lambda k=k: down_arrived(k, y))
        start(go_up, lambda k=k: down(k, d_up.at[k], up, y))
        start(go_dn, lambda k=k: down(k, d_dn.at[k], dn, y))
        for i in range(Y - 1):
            start(None, lambda k=k, i=i: down(k, d_y.at[i, k], across[i], y))

    for zs in range(Z):
        for o in others:
            for k, a in pieces:
                if k < detour:
                    when(zs != z, lambda a=a, k=k, zs=zs, o=o: arrived(a, k, zs * Y + o))
                else:
                    arrived(a, k, zs * Y + o)
    units = wg.shape[1]
    width = 256 if units % 256 == 0 else 128

    @pl.loop(0, units // width)
    def _(j):
        at = pl.ds(pl.multiple_of(j * width, width), width)
        gate = jnp.dot(normed[...], wg[:, at], preferred_element_type=jnp.float32)
        up_ = jnp.dot(normed[...], wu[:, at], preferred_element_type=jnp.float32)
        hidden[:, at] = (gate / (1.0 + jnp.exp(-gate)) * up_).astype(jnp.bfloat16)

    for o in others:
        for k in range(nd):
            down_arrived(k, o)
    for cond, make in sent:
        if cond is None:
            make().wait_send()
        else:
            when(cond, lambda make=make: make().wait_send())


def gather(mesh, g, u, d, x):
    fs, T = mesh.shape["fs"], mesh.shape["tp"]
    Z, Y = lines(fs)
    rows, rows_d = g.shape[0], d.shape[0]
    nk = max(1, min(4, rows // 64))
    nd = max(1, min(16, rows_d // 48))
    detour = nk // 2 if Y == 2 else 0
    dma = pltpu.SemaphoreType.DMA
    vmem = pl.BlockSpec(memory_space=pltpu.VMEM)
    return pl.pallas_call(
        functools.partial(gather_kernel, Z, Y, T, nk, nd, detour),
        out_shape=(
            jax.ShapeDtypeStruct((rows * fs, g.shape[1]), g.dtype),
            jax.ShapeDtypeStruct((rows * fs, g.shape[1]), g.dtype),
            jax.ShapeDtypeStruct((rows_d * Y, d.shape[1] * T), d.dtype),
            jax.ShapeDtypeStruct((x.shape[0], g.shape[1]), d.dtype),
        ),
        in_specs=[vmem] * 4,
        out_specs=[vmem] * 4,
        scratch_shapes=[
            pltpu.VMEM(x.shape, x.dtype),
            dma((Z, 2, nk)), dma((Z, 2, nk)), dma((max(Y - 1, 1), Z, 2, nk)), dma((fs, 2, nk)),
            dma((2, 2, nk)), dma((nd,)), dma((nd,)), dma((max(Y - 1, 1), nd)), dma((Y, nd)),
            dma((1,)), dma((T,)),
        ],
        compiler_params=pltpu.CompilerParams(
            collective_id=0, has_side_effects=True, vmem_limit_bytes=GRANT
        ),
        name="gather",
    )(g, u, d, x)


def layer_kernel(T, h_ref, wg, wu, wd, part, og, ou, od, sems):
    outs = [pltpu.make_async_copy(s, d, sems.at[i]) for i, (s, d) in enumerate(((wg, og), (wu, ou), (wd, od)))]
    for c in outs:
        c.start()
    width = part.shape[1] // T

    @pl.loop(0, T)
    def _(j):
        at = pl.ds(pl.multiple_of(j * width, width), width)
        part[:, at] = jnp.dot(h_ref[...], wd[:, at], preferred_element_type=jnp.float32).astype(jnp.bfloat16)

    for c in outs:
        c.wait()


def layer(mesh, h, wg, wu, wd):
    vmem, any_ = pl.BlockSpec(memory_space=pltpu.VMEM), pl.BlockSpec(memory_space=pl.ANY)
    return pl.pallas_call(
        functools.partial(layer_kernel, mesh.shape["tp"]),
        out_shape=(
            jax.ShapeDtypeStruct((h.shape[0], wd.shape[1]), jnp.bfloat16),
            jax.ShapeDtypeStruct(wg.shape, wg.dtype),
            jax.ShapeDtypeStruct(wu.shape, wu.dtype),
            jax.ShapeDtypeStruct(wd.shape, wd.dtype),
        ),
        in_specs=[vmem] * 4,
        out_specs=[vmem] + [any_] * 3,
        scratch_shapes=[pltpu.SemaphoreType.DMA((3,))],
        compiler_params=pltpu.CompilerParams(vmem_limit_bytes=GRANT),
        name="layer",
    )(h, wg, wu, wd)


def sum_kernel(X, nc, p_ref, o_ref, near, pair, far, s_a, r_a, s_b, r_b):
    f, t = lax.axis_index("fs"), lax.axis_index("tp")
    x, core = t // 2, lax.rem(t, 2)
    mate = (f, x * 2 + 1 - core)
    n, width = o_ref.shape
    h = n // nc
    barrier = pltpu.get_barrier_semaphore()
    xs = [lax.rem(x + i, X) for i in range(1, X)]
    peers = [mate] + [(f, q * 2 + core) for q in xs]
    for dev in peers:
        pl.semaphore_signal(barrier, inc=1, device_id=dev, device_id_type=MESH)
    pl.semaphore_wait(barrier, len(peers))

    order = [(c, i) for c in range(nc) for i in list(range(1, X)) + [0]]

    def block(c, i, which):
        q = lax.rem(x + i, X)
        start = pl.multiple_of((q * 2 + which) * width, width)
        return p_ref.at[pl.ds(c * h, h), pl.ds(start, width)]

    def to_mate(c, i):
        return pltpu.make_async_remote_copy(
            src_ref=block(c, i, 1 - core), dst_ref=near.at[i, pl.ds(c * h, h), :],
            send_sem=s_a.at[i, c], recv_sem=r_a.at[i, c], device_id=mate, device_id_type=MESH,
        )

    def to_far(c, i):
        return pltpu.make_async_remote_copy(
            src_ref=pair.at[i, pl.ds(c * h, h), :], dst_ref=far.at[i, pl.ds(c * h, h), :],
            send_sem=s_b.at[i, c], recv_sem=r_b.at[i, c], device_id=peers[i], device_id_type=MESH,
        )

    order = [(c, i) for c in range(nc) for i in range(1, X)]
    for c, i in order:
        to_mate(c, i).start()
    for c in range(nc):
        to_mate(c, 0).start()
    for c, i in order:
        to_mate(c, i).wait_recv()
        pair[i, pl.ds(c * h, h), :] = (
            block(c, i, core)[...].astype(jnp.float32) + near[i, pl.ds(c * h, h), :].astype(jnp.float32)
        ).astype(jnp.bfloat16)
        to_far(c, i).start()
    for c in range(nc):
        to_mate(c, 0).wait_recv()
        acc = block(c, 0, core)[...].astype(jnp.float32) + near[0, pl.ds(c * h, h), :].astype(jnp.float32)
        for i in range(1, X):
            to_far(c, i).wait_recv()
            acc = acc + far[i, pl.ds(c * h, h), :].astype(jnp.float32)
        o_ref[pl.ds(c * h, h), :] = acc.astype(o_ref.dtype)
    for c in range(nc):
        for i in range(X):
            to_mate(c, i).wait_send()
            if i:
                to_far(c, i).wait_send()


def sum_parts(mesh, p):
    T = mesh.shape["tp"]
    X = T // 2
    n, width = p.shape[0], p.shape[1] // T
    nc = 4
    dma = pltpu.SemaphoreType.DMA
    vmem = pl.BlockSpec(memory_space=pltpu.VMEM)
    return pl.pallas_call(
        functools.partial(sum_kernel, X, nc),
        out_shape=jax.ShapeDtypeStruct((n, width), jnp.bfloat16),
        in_specs=[vmem],
        out_specs=vmem,
        scratch_shapes=[pltpu.VMEM((X, n, width), jnp.bfloat16)] * 3 + [dma((X, nc))] * 4,
        compiler_params=pltpu.CompilerParams(
            collective_id=1, has_side_effects=True, vmem_limit_bytes=16 * 1024 * 1024
        ),
        name="sum_parts",
    )(p)


def solution(mesh):
    def on_device(tokens, norm_gain, gate_weight, up_weight, down_weight):
        row_gain = norm_gain[:, None]
        gate_local = (row_gain * gate_weight).astype(jnp.bfloat16)
        up_local = (row_gain * up_weight).astype(jnp.bfloat16)
        down_local = down_weight.astype(jnp.bfloat16)
        wg, wu, wd, hidden = gather(mesh, gate_local, up_local, down_local, tokens)
        part, og, ou, od = layer(mesh, hidden, wg, wu, wd)
        return (sum_parts(mesh, part), og, ou, od)

    return jax.shard_map(
        on_device,
        mesh=mesh,
        in_specs=(P("fs", None), P("fs"), P("fs", "tp"), P("fs", "tp"), P("fs", "tp")),
        out_specs=(P("fs", "tp"), P(None, "tp"), P(None, "tp"), P("tp", None)),
        check_vma=False,
    )
```

profile of v0, /device:TPU:0, one launch (start us, length us, event | category | flops | bytes accessed | tf_op | source)
XLA Modules:
  0.0 228.0 jit_solution(4000525347265651649)
XLA Ops:
  0.6 0.0 copy-start.1
  0.6 0.0 copy-start.2
  0.7 1.6 convert_element_type.11.d_ref
  2.3 0.2 copy-done.1
  2.5 0.0 copy-done.2
  2.5 0.0 copy-start
  2.5 2.0 multiply_convert_fusion
  4.5 0.1 copy-done
  4.6 199.5 %gather.1 = (bf16[2048,1536]{1,0:T(8,128)(2,1)S(1)}, bf16[2048,1536]{1,0:T(8,128)(2,1)S(1)}, bf16[1536,2048]{1,0:T(8,128)(2,1)S(1)}, bf16[512,1536]{1,0:T(8,128)(2,1)S(1)}) custom-call(bf16[256,1536]{1,0:T(8,128)(2,1)S(1)} %get-tuple-element.21.g_ref, bf16[256,1536]{1,0:T(8,128)(2,1)S(1)} %get-tuple-element.20.u_ref, ...), custom_call_target="tpu_custom_call" | custom-call | tf_op jit(solution)/shard_map/gather/pallas_call | solution.py:201
  204.0 6.7 %layer.1 = (bf16[512,2048]{1,0:T(8,128)(2,1)S(1)}, bf16[2048,1536]{1,0:T(8,128)(2,1)}, bf16[2048,1536]{1,0:T(8,128)(2,1)}, bf16[1536,2048]{1,0:T(8,128)(2,1)}) custom-call(bf16[512,1536]{1,0:T(8,128)(2,1)S(1)} %get-tuple-element.12.h_ref, bf16[2048,1536]{1,0:T(8,128)(2,1)S(1)} %get-tuple-element.13.wg, bf16[2048,1536]{1,0:T(8,128)(2,1)S(1)} %get-tuple-element.14.wu, ...), custom_call_target="tpu_custom_call" | custom-call | tf_op jit(solution)/shard_map/layer/pallas_call | solution.py:241
  210.7 16.4 %sum_parts.1 = bf16[512,512]{1,0:T(8,128)(2,1)S(1)} custom-call(bf16[512,2048]{1,0:T(8,128)(2,1)S(1)} %get-tuple-element.16.p_ref), custom_call_target="tpu_custom_call" | custom-call | tf_op jit(solution)/shard_map/sum_parts/pallas_call | solution.py:321
  227.2 0.8 copy.10
Async XLA Ops:
  0.6 1.9 copy-start.1
  0.6 1.9 copy-start.2
  2.5 2.1 copy-start
where the time goes:
time: 228 us
  Pallas kernels  223 us (98%)
  other arithmetic  3.59 us (2%)
    pallas_call x1, Pallas kernels, gather(): pl.pallas_call(functools.partial(gather_kernel, Z, Y, T, nk, nd, detour),...  199 us
    pallas_call x1, Pallas kernels, sum_parts(): pl.pallas_call(functools.partial(sum_kernel, X, nc), out_shape=jax.ShapeD...  16.4 us
    pallas_call x1, Pallas kernels, layer(): pl.pallas_call(functools.partial(layer_kernel, mesh.shape['tp']), out_sha...  6.69 us

commit v1 on v0

v1 whole, which is shorter than its diff:
```python
import functools

import jax
import jax.numpy as jnp
from jax import lax
from jax.experimental import pallas as pl
from jax.experimental.pallas import tpu as pltpu
from jax.sharding import PartitionSpec as P

MESH = pl.DeviceIdType.MESH
GRANT = 26 * 1024 * 1024
W = 128
LAG = 4
ORDER = (5, 0, 2, 6, 1, 3, 4, 7)


def lines(fs):
    y = 1
    while 2 * (2 * y) * (2 * y) <= fs:
        y *= 2
    return fs // y, y


def when(cond, fn):
    pl.when(cond)(fn)


def each(lo, hi, fn):
    if hi > lo:
        pl.loop(lo, hi)(fn)


def layer_kernel(
    Z, Y, T, nk, paired,
    gain_hbm, g_hbm, u_hbm, d_hbm, x_hbm,
    wg, wu, wd, mixed,
    gain_row, stage_g, stage_u, stage_d, own_d, transit, normed, hidden, part, near, pair, far,
    in_gain, in_g, in_u, in_d, in_x, s_up, s_dn, s_y, s_det, r_w, s_one, s_tz, s_tx, r_t,
    s_dz, s_dy, r_d, s_a, r_a, s_b, r_b,
):
    f, t = lax.axis_index("fs"), lax.axis_index("tp")
    X = T // 2
    z, y = f // Y, lax.rem(f, Y)
    x, core = t // 2, lax.rem(t, 2)
    has_up, has_dn = z < Z - 1, z > 0
    up, dn = (f + Y, t), (f - Y, t)
    others = [lax.rem(y + i, Y) for i in range(1, Y)]
    across = [(z * Y + o, t) for o in others]
    rows = g_hbm.shape[0]
    ck = rows // nk
    rows_d, cols_d = d_hbm.shape
    pq = cols_d // W
    nc = T * pq
    n = x_hbm.shape[0]
    staged, full = (stage_g, stage_u), (wg, wu)
    pieces = [(k, a) for k in range(nk) for a in range(2)]

    def load(k, a):
        at = pl.ds(k * ck, ck)
        return pltpu.make_async_copy((g_hbm, u_hbm)[a].at[at, :], staged[a].at[at, :], (in_g, in_u)[a].at[k])

    load_d = pltpu.make_async_copy(d_hbm, stage_d, in_d.at[0])
    load_x = pltpu.make_async_copy(x_hbm, normed, in_x.at[0])
    load_gain = pltpu.make_async_copy(gain_hbm, gain_row, in_gain.at[0])
    load_gain.start()
    for k, a in pieces:
        load(k, a).start()
    load_d.start()
    load_x.start()

    barrier = pltpu.get_barrier_semaphore()

    def greet(dev):
        pl.semaphore_signal(barrier, inc=1, device_id=dev, device_id_type=MESH)

    when(has_up, lambda: greet(up))
    when(has_dn, lambda: greet(dn))
    for dev in across:
        greet(dev)
    for i in range(1, T):
        greet((f, lax.rem(t + i, T)))

    load_gain.wait()
    diagonal = lax.broadcasted_iota(jnp.int32, (rows, rows), 0) == lax.broadcasted_iota(jnp.int32, (rows, rows), 1)
    gain = jnp.sum(jnp.where(diagonal, jnp.broadcast_to(gain_row[...], (rows, rows)), 0.0), axis=1, keepdims=True)

    def copy(src, dst, ss, rs, dev):
        return pltpu.make_async_remote_copy(
            src_ref=src, dst_ref=dst, send_sem=ss, recv_sem=rs, device_id=dev, device_id_type=MESH
        )

    def weight(a, k, source, ss, dev):
        at = full[a].at[pl.ds(pl.multiple_of(source * rows + k * ck, ck), ck), :]
        return copy(at, at, ss, r_w.at[source, a, k], dev)

    def arrived(a, k, source):
        weight(a, k, source, s_det.at[a, k], (f, lax.rem(t + 1, T))).wait_recv()

    sent = []

    def start(cond, make):
        sent.append((cond, make))
        if cond is None:
            make().start()
        else:
            when(cond, lambda: make().start())

    def scale(k, a):
        load(k, a).wait()
        at = pl.ds(pl.multiple_of(f * rows + k * ck, ck), ck)
        full[a][at, :] = (gain[k * ck:(k + 1) * ck, :] * staged[a][pl.ds(k * ck, ck), :]).astype(jnp.bfloat16)

    def send_own(k, a):
        start(has_up, lambda: weight(a, k, f, s_up.at[z, a, k], up))
        start(has_dn, lambda: weight(a, k, f, s_dn.at[z, a, k], dn))
        for i in range(Y - 1):
            start(None, lambda i=i: weight(a, k, f, s_y.at[i, z, a, k], across[i]))

    scale(*pieces[0])
    scale(*pieces[1])
    pl.semaphore_wait(barrier, Y + T - 2 + has_up.astype(jnp.int32) + has_dn.astype(jnp.int32))
    for i, piece in enumerate(pieces):
        if i + 2 < len(pieces):
            scale(*pieces[i + 2])
        send_own(*piece)

    def cols(j):
        return pl.ds(pl.multiple_of(j * W, W), W)

    def line_rows(line):
        return pl.ds(pl.multiple_of(line * rows_d, rows_d), rows_d)

    def down(line, j, ss, dev):
        at = wd.at[line_rows(line), cols(j)]
        return copy(at, at, ss, r_d.at[line, j], dev)

    def down_arrived(line, j):
        down(line, j, s_dy.at[0, j], (f, lax.rem(t + 1, T))).wait_recv()

    load_d.wait()
    own_d[...] = stage_d[...].astype(jnp.bfloat16)

    @pl.when(z == t)
    def _():
        wd[line_rows(y), pl.ds(pl.multiple_of(t * cols_d, cols_d), cols_d)] = stage_d[...].astype(jnp.bfloat16)

    def first(p):
        return copy(
            own_d.at[:, pl.ds(p * W, W)], wd.at[line_rows(y), cols(t * pq + p)],
            s_one.at[p], r_d.at[y, t * pq + p], (f, z),
        )

    load_x.wait()
    slab = 64 if n % 64 == 0 else n

    def normalise(i):
        at = pl.ds(pl.multiple_of(i * slab, slab), slab)
        v = normed[at, :].astype(jnp.float32)
        normed[at, :] = (v * lax.rsqrt(jnp.mean(v * v, axis=1, keepdims=True) + 1e-05)).astype(jnp.bfloat16)

    normalise(0)
    for p in range(pq):
        start(z != t, lambda p=p: first(p))
    each(1, n // slab, normalise)

    at_home = z == t
    can_up = jnp.logical_and(has_up, z >= t)
    can_dn = jnp.logical_and(has_dn, z <= t)
    inner = jnp.logical_and(has_up, has_dn)
    if paired:
        half = t // (T // 2)
        shift = (nc // 2) * (1 - half)
        far_up, far_dn = half == 0, half == 1
        beyond = jnp.logical_or(jnp.logical_and(z < t, far_dn), jnp.logical_and(z > t, far_up))
        fwd_mid = jnp.logical_or(
            jnp.logical_and(can_up, jnp.logical_not(far_up)), jnp.logical_and(can_dn, jnp.logical_not(far_dn))
        )
        mid_lo, mid_hi = 2 * pq, 2 * pq + pq // 2
    else:
        shift = 0
        mid_lo, mid_hi = 0, nc
    fwd_all = jnp.logical_or(can_up, can_dn)
    away = jnp.logical_not(at_home)

    def column(r):
        return lax.rem(r + shift, nc)

    bent = (pq if paired else 0, lambda i: column(core * pq + i))
    low = (pq if paired else 0, lambda i: column((1 - core) * pq + i))
    mid = (mid_hi - mid_lo, lambda i: column(mid_lo + i))
    high = (nc - mid_hi, lambda i: column(mid_hi + i))

    def over(kind, fn):
        each(0, kind[0], lambda i: fn(kind[1](i)))

    def both(a, b):
        return jnp.logical_and(a, b)

    def z_send(line, j, which, direction):
        return down(line, j, s_dz.at[direction, which, j], (up, dn)[direction])

    def near_ok(direction):
        return jnp.logical_not((far_up, far_dn)[direction])

    def can(direction):
        return (can_up, can_dn)[direction]

    def cross(j):
        for i in range(Y - 1):
            down(y, j, s_dy.at[i, j], across[i]).start()

    other = others[0]

    def assemble():
        for i in range(1, T):
            owner = lax.rem(t + i, T)
            for p in range(pq):
                down_arrived(y, owner * pq + p)
        over(high, cross)
        if paired:
            @pl.when(inner)
            def _():
                over(low, cross)
                over(mid, cross)

    if paired:
        guest = lax.rem(t + T // 2, T)
        guest_dn = guest // (T // 2) == 1
        guest_here = jnp.logical_or(both(z < guest, guest_dn), both(z > guest, jnp.logical_not(guest_dn)))
        guest_on = (both(both(z >= guest, has_up), jnp.logical_not(guest_dn)), both(both(z <= guest, has_dn), guest_dn))

        def relay(p, direction, src):
            return copy(
                src.at[:, cols(p)], transit.at[:, cols(p)], s_tz.at[p], r_t.at[p], (up, dn)[direction]
            )

        def hand_over(p):
            return copy(
                transit.at[:, cols(p)], wd.at[line_rows(y), cols(t * pq + p)], s_tx.at[p], r_d.at[y, t * pq + p], (f, guest)
            )

    def leave(direction):
        if paired:
            @pl.when(both(z == guest, guest_on[direction]))
            def _():
                each(0, pq, lambda p: relay(p, direction, own_d).start())

        @pl.when(both(at_home, can(direction)))
        def _():
            if paired:
                @pl.when(near_ok(direction))
                def _():
                    over(bent, lambda j: z_send(y, j, 0, direction).start())
            for kind in (low, mid, high):
                over(kind, lambda j: z_send(y, j, 0, direction).start())

    def hook(s):
        when(z == s, lambda: leave(0))
        when(z == Z - 1 - s, lambda: leave(1))

    for step in range(1, Z):
        for count, (k, a) in enumerate(pieces):
            if step == 1 and count == len(pieces) // 2:
                when(at_home, assemble)
            for sign in (-1, 1):
                zs = z + sign * step
                source = zs * Y + y
                valid = zs >= 0 if sign < 0 else zs < Z
                onward = jnp.logical_and(valid, has_up if sign < 0 else has_dn)
                when(valid, lambda a=a, k=k, s=source: arrived(a, k, s))
                if sign < 0:
                    start(onward, lambda a=a, k=k, s=source, q=zs: weight(a, k, s, s_up.at[q, a, k], up))
                else:
                    start(onward, lambda a=a, k=k, s=source, q=zs: weight(a, k, s, s_dn.at[q, a, k], dn))
                crossing = valid
                if paired and step == 1:
                    crossing = both(valid, zs != (0 if sign < 0 else Z - 1))
                for i in range(Y - 1):
                    start(crossing, lambda a=a, k=k, s=source, q=zs, i=i: weight(a, k, s, s_y.at[i, q, a, k], across[i]))
        if step == 1:
            hook(0)
            if paired:
                ends = jnp.logical_not(inner)
                beside = across[0][0]
                for k, a in pieces:
                    when(ends, lambda a=a, k=k: arrived(a, k, beside))
                    start(both(ends, has_up), lambda a=a, k=k: weight(a, k, beside, s_det.at[a, k], up))
                    start(both(ends, has_dn), lambda a=a, k=k: weight(a, k, beside, s_det.at[a, k], dn))
        hook(step)

    if paired:
        @pl.when(at_home)
        def _():
            @pl.when(jnp.logical_not(inner))
            def _():
                over(low, cross)
                over(mid, cross)
            over(bent, cross)

    else:
        when(at_home, lambda: over(mid, cross))

    if paired:
        @pl.when(guest_here)
        def _():
            def pass_on(p):
                copy(
                    transit.at[:, cols(p)], transit.at[:, cols(p)], s_tz.at[p], r_t.at[p], (f, guest)
                ).wait_recv()
                for direction in range(2):
                    when(guest_on[direction], lambda: relay(p, direction, transit).start())
                hand_over(p).start()
            each(0, pq, pass_on)

    @pl.when(away)
    def _():
        def bend(j):
            down_arrived(y, j)
            for direction in range(2):
                when(both(can(direction), near_ok(direction)), lambda: z_send(y, j, 0, direction).start())
            cross(j)

        def straight(j):
            down_arrived(y, j)
            for direction in range(2):
                when(can(direction), lambda: z_send(y, j, 0, direction).start())
            if paired:
                when(beyond, lambda: cross(j))
            else:
                cross(j)

        over(bent, bend)
        over(low, straight)
        over(mid, straight)

    if paired:
        @pl.when(fwd_mid)
        def _():
            def twin(j):
                down_arrived(other, j)
                for direction in range(2):
                    when(both(can(direction), near_ok(direction)), lambda: z_send(other, j, 1, direction).start())
            over(low, twin)
            over(mid, twin)

        @pl.when(fwd_all)
        def _():
            def twins(j):
                @pl.when(away)
                def _():
                    down_arrived(y, j)
                    for direction in range(2):
                        when(can(direction), lambda: z_send(y, j, 0, direction).start())
                down_arrived(other, j)
                for direction in range(2):
                    when(can(direction), lambda: z_send(other, j, 1, direction).start())
            over(high, twins)

    for zs in range(Z):
        for o in others:
            for k, a in pieces:
                if paired and zs in (0, Z - 1):
                    when(zs != z, lambda a=a, k=k, zs=zs, o=o: arrived(a, k, zs * Y + o))
                else:
                    arrived(a, k, zs * Y + o)
    units = wg.shape[1]
    width = 256 if units % 256 == 0 else 128

    @pl.loop(0, units // width)
    def _(j):
        at = pl.ds(pl.multiple_of(j * width, width), width)
        gate = jnp.dot(normed[...], wg[:, at], preferred_element_type=jnp.float32)
        up_ = jnp.dot(normed[...], wu[:, at], preferred_element_type=jnp.float32)
        hidden[:, at] = (gate / (1.0 + jnp.exp(-gate)) * up_).astype(jnp.bfloat16)

    for cond, make in sent:
        if cond is None:
            make().wait_send()
        else:
            when(cond, lambda make=make: make().wait_send())

    mate = (f, x * 2 + 1 - core)

    def piece_of(i):
        if not paired:
            return i
        eighth = sum(g * (i // (nc // 8) == e).astype(jnp.int32) for e, g in enumerate(ORDER))
        r = eighth * (nc // 8) + lax.rem(i, nc // 8)
        return lax.rem(r + (nc // 2) * (z >= Z // 2).astype(jnp.int32), nc)

    def to_mate(j):
        return copy(part.at[:, cols(j)], near.at[:, cols(j)], s_a.at[j], r_a.at[j], mate)

    def to_owner(j):
        owner = j // pq
        slot = lax.rem(x - owner // 2 + X, X) - 1
        p = lax.rem(j, pq)
        return copy(pair.at[:, cols(j)], far.at[slot, :, cols(p)], s_b.at[j], r_b.at[slot, p], (f, owner))

    def product(i):
        j = piece_of(i)
        if paired:
            r = lax.rem(j - shift + nc, nc)
            is_high = r >= mid_hi
            is_bent = both(r < 2 * pq, r // pq == core)
            is_mid = jnp.logical_not(jnp.logical_or(is_high, is_bent))
            late = both(is_high, jnp.logical_not(fwd_all))
            when(both(late, away), lambda: down_arrived(y, j))
            late_other = jnp.logical_or(jnp.logical_or(late, is_bent), both(is_mid, jnp.logical_not(fwd_mid)))
            when(late_other, lambda: down_arrived(other, j))
        else:
            for o in others:
                down_arrived(o, j)
        part[:, cols(j)] = jnp.dot(hidden[...], wd[:, cols(j)], preferred_element_type=jnp.float32).astype(jnp.bfloat16)

    def ours(j):
        return lax.rem(j // pq, 2) == core

    def at_owner_chip(j):
        return j // pq // 2 == x

    @pl.loop(0, nc + LAG)
    def _(i):
        now = i < nc
        last = both(i >= 1, i <= nc)
        done = i >= LAG
        j0 = piece_of(jnp.minimum(i, nc - 1))
        j1 = piece_of(jnp.minimum(jnp.maximum(i - 1, 0), nc - 1))
        j2 = piece_of(jnp.maximum(i - LAG, 0))
        when(now, lambda: product(i))
        mine = both(last, ours(j1))
        ship = both(mine, jnp.logical_not(at_owner_chip(j1)))
        when(mine, lambda: to_mate(j1).wait_recv())

        @pl.when(ship)
        def _():
            pair[:, cols(j1)] = (
                part[:, cols(j1)].astype(jnp.float32) + near[:, cols(j1)].astype(jnp.float32)
            ).astype(jnp.bfloat16)

        when(both(now, jnp.logical_not(ours(j0))), lambda: to_mate(j0).start())

        @pl.when(both(done, j2 // pq == t))
        def _():
            p = lax.rem(j2, pq)
            acc = part[:, cols(j2)].astype(jnp.float32) + near[:, cols(j2)].astype(jnp.float32)
            for slot in range(X - 1):
                copy(
                    pair.at[:, cols(j2)], far.at[slot, :, cols(p)], s_b.at[j2], r_b.at[slot, p], mate
                ).wait_recv()
                acc = acc + far[slot, :, cols(p)].astype(jnp.float32)
            mixed[:, cols(p)] = acc.astype(mixed.dtype)

        when(ship, lambda: to_owner(j1).start())

    if paired:
        def relayed(p):
            for direction in range(2):
                when(guest_on[direction], lambda: relay(p, direction, transit).wait_send())
            when(guest_here, lambda: hand_over(p).wait_send())
        each(0, pq, relayed)

    def crossed(j):
        for i in range(Y - 1):
            down(y, j, s_dy.at[i, j], across[i]).wait_send()

    def left(line, which, allowed):
        def fn(j):
            for direction in range(2):
                when(allowed(direction), lambda: z_send(line, j, which, direction).wait_send())
        return fn

    if paired:
        over(bent, left(y, 0, lambda d: both(can(d), near_ok(d))))
        for kind in (low, mid):
            over(kind, left(other, 1, lambda d: both(can(d), near_ok(d))))
        over(high, left(other, 1, can))
        over(bent, crossed)
        for kind in (low, mid):
            when(jnp.logical_or(at_home, beyond), lambda kind=kind: over(kind, crossed))
        when(at_home, lambda: over(high, crossed))
    else:
        over(mid, crossed)
    for kind in (low, mid, high):
        over(kind, left(y, 0, can))

    def swept(j):
        when(jnp.logical_not(ours(j)), lambda: to_mate(j).wait_send())
        when(both(ours(j), jnp.logical_not(at_owner_chip(j))), lambda: to_owner(j).wait_send())
    each(0, nc, swept)


def layer(mesh, gain, g, u, d, x):
    fs, T = mesh.shape["fs"], mesh.shape["tp"]
    Z, Y = lines(fs)
    X = T // 2
    rows, rows_d, n = g.shape[0], d.shape[0], x.shape[0]
    pq = d.shape[1] // W
    nc = T * pq
    nk = max(1, min(4, rows // 64))
    paired = Y == 2 and X == 2 and Z == T and pq % 2 == 0
    lanes = max(Y - 1, 1)
    dma = pltpu.SemaphoreType.DMA
    vmem, hbm = pl.BlockSpec(memory_space=pltpu.VMEM), pl.BlockSpec(memory_space=pltpu.HBM)
    bf = jnp.bfloat16
    return pl.pallas_call(
        functools.partial(layer_kernel, Z, Y, T, nk, paired),
        out_shape=(
            jax.ShapeDtypeStruct((rows * fs, g.shape[1]), bf),
            jax.ShapeDtypeStruct((rows * fs, g.shape[1]), bf),
            jax.ShapeDtypeStruct((rows_d * Y, d.shape[1] * T), bf),
            jax.ShapeDtypeStruct((n, d.shape[1]), bf),
        ),
        in_specs=[hbm] * 5,
        out_specs=[vmem] * 4,
        scratch_shapes=[
            pltpu.VMEM(gain.shape, jnp.float32),
            pltpu.VMEM(g.shape, jnp.float32), pltpu.VMEM(u.shape, jnp.float32), pltpu.VMEM(d.shape, jnp.float32),
            pltpu.VMEM(d.shape, bf), pltpu.VMEM(d.shape, bf), pltpu.VMEM(x.shape, bf), pltpu.VMEM((n, g.shape[1]), bf),
            pltpu.VMEM((n, nc * W), bf), pltpu.VMEM((n, nc * W), bf), pltpu.VMEM((n, nc * W), bf),
            pltpu.VMEM((max(X - 1, 1), n, pq * W), bf),
            dma((1,)), dma((nk,)), dma((nk,)), dma((1,)), dma((1,)),
            dma((Z, 2, nk)), dma((Z, 2, nk)), dma((lanes, Z, 2, nk)), dma((2, nk)), dma((fs, 2, nk)),
            dma((pq,)), dma((pq,)), dma((pq,)), dma((pq,)),
            dma((2, 2, nc)), dma((lanes, nc)), dma((Y, nc)),
            dma((nc,)), dma((nc,)), dma((nc,)), dma((max(X - 1, 1), pq)),
        ],
        compiler_params=pltpu.CompilerParams(
            collective_id=0, has_side_effects=True, vmem_limit_bytes=GRANT
        ),
        name="layer",
    )(*(pltpu.with_memory_space_constraint(v, pltpu.HBM) for v in (gain, g, u, d, x)))


def publish_kernel(wg, wu, wd, mixed, og, ou, od, om, sems):
    outs = [
        pltpu.make_async_copy(s, d, sems.at[i])
        for i, (s, d) in enumerate(((wg, og), (wu, ou), (wd, od), (mixed, om)))
    ]
    for c in outs:
        c.start()
    for c in outs:
        c.wait()


def publish(*arrays):
    vmem, any_ = pl.BlockSpec(memory_space=pltpu.VMEM), pl.BlockSpec(memory_space=pl.ANY)
    return pl.pallas_call(
        publish_kernel,
        out_shape=tuple(jax.ShapeDtypeStruct(a.shape, a.dtype) for a in arrays),
        in_specs=[vmem] * 4,
        out_specs=[any_] * 4,
        scratch_shapes=[pltpu.SemaphoreType.DMA((4,))],
        compiler_params=pltpu.CompilerParams(vmem_limit_bytes=1024 * 1024),
        name="publish",
    )(*arrays)


def solution(mesh):
    def on_device(tokens, norm_gain, gate_weight, up_weight, down_weight):
        wg, wu, wd, mixed = layer(mesh, norm_gain[None, :], gate_weight, up_weight, down_weight, tokens)
        og, ou, od, om = publish(wg, wu, wd, mixed)
        return (om, og, ou, od)

    return jax.shard_map(
        on_device,
        mesh=mesh,
        in_specs=(P("fs", None), P("fs"), P("fs", "tp"), P("fs", "tp"), P("fs", "tp")),
        out_specs=(P("fs", "tp"), P(None, "tp"), P(None, "tp"), P("tp", None)),
        check_vma=False,
    )
```

time: 228 us -> 217 us (0.952); the launches traced: 228 us -> 214 us
  Pallas kernels: 223 us -> 214 us
  other arithmetic: 3.59 us -> 0 us
    pallas_call x3 -> x2, Pallas kernels: 223 us -> 214 us  [the longest x1 207 us: layer(): pl.pallas_call(functools.partial(layer_kernel, Z, Y, T, nk, paired), out_...]
    convert_element_type x2 -> x0, other arithmetic: 3.59 us -> none  [the longest x1 1.97 us: on_device(): up_local = (row_gain * up_weight).astype(jnp.bfloat16)]
where the time goes in v1:
time: 217 us; the launch traced here: 214 us
  Pallas kernels  214 us (99%)
    pallas_call x1, Pallas kernels, layer(): pl.pallas_call(functools.partial(layer_kernel, Z, Y, T, nk, paired), out_...  207 us
    pallas_call x1, Pallas kernels, publish(): pl.pallas_call(publish_kernel, out_shape=tuple((jax.ShapeDtypeStruct(a.sh...  6.71 us

profile of v1, /device:TPU:0, one launch (start us, length us, event | category | flops | bytes accessed | tf_op | source)
XLA Modules:
  0.0 214.4 jit_solution(14501240889692498085)
XLA Ops:
  0.6 207.1 %layer.1 = (bf16[2048,1536]{1,0:T(8,128)(2,1)S(1)}, bf16[2048,1536]{1,0:T(8,128)(2,1)S(1)}, bf16[1536,2048]{1,0:T(8,128)(2,1)S(1)}, bf16[512,512]{1,0:T(8,128)(2,1)S(1)}) custom-call(f32[1,256]{1,0:T(1,128)} %bitcast.1, f32[256,1536]{1,0:T(8,128)} %g_hbm.1, f32[256,1536]{1,0:T(8,128)} %u_hbm.1, f32[768,512]{1,0:T(8,128)} %d_hbm.1, bf16[512,2048]{1,0:T(8,128)(2,1)} %x_hbm.1), custom_call_target="tpu_custom_call" | custom-call | tf_op jit(solution)/shard_map/layer/pallas_call | solution.py:506
  207.7 6.7 %publish.1 = (bf16[2048,1536]{1,0:T(8,128)(2,1)}, bf16[2048,1536]{1,0:T(8,128)(2,1)}, bf16[1536,2048]{1,0:T(8,128)(2,1)}, bf16[512,512]{1,0:T(8,128)(2,1)}) custom-call(bf16[2048,1536]{1,0:T(8,128)(2,1)S(1)} %get-tuple-element.12.wg, bf16[2048,1536]{1,0:T(8,128)(2,1)S(1)} %get-tuple-element.13.wu, bf16[1536,2048]{1,0:T(8,128)(2,1)S(1)} %get-tuple-element.14.wd, ...), custom_call_target="tpu_custom_call" | custom-call | tf_op jit(solution)/shard_map/publish/pallas_call | solution.py:548

commit v2 on v1

v2 whole, which is shorter than its diff:
```python
import functools

import jax
import jax.numpy as jnp
from jax import lax
from jax.experimental import pallas as pl
from jax.experimental.pallas import tpu as pltpu
from jax.sharding import PartitionSpec as P

MESH = pl.DeviceIdType.MESH
GRANT = 26 * 1024 * 1024
CUTS = 4
W = 128


def lines(fs):
    y = 1
    while 2 * (2 * y) * (2 * y) <= fs:
        y *= 2
    return fs // y, y


def when(cond, fn):
    pl.when(cond)(fn)


def each(lo, hi, fn):
    if hi > lo:
        pl.loop(lo, hi)(fn)


def column_times(pq):
    tail = 4 * pq - 2 * pq - pq // 2
    return (
        [18 + 2 * (p % pq + 1) / pq for p in range(2 * pq)]
        + [20 + (i + 1) / (pq // 2) for i in range(pq // 2)]
        + [15 + 6 * (i + 1) / tail for i in range(tail)]
    )


def column_units(pq, nc, paired):
    times = column_times(pq) if paired else range(nc)
    if pq % 2:
        return (), tuple(sorted(range(nc), key=lambda p: times[p]))
    pairs = sorted(range(0, nc, 2), key=lambda p: max(times[p], times[p + 1]))
    ends = [p + i for p in pairs[-2:] for i in range(2)]
    return tuple(pairs[:-2]), tuple(sorted(ends, key=lambda p: times[p]))


def layer_kernel(
    Z, Y, T, nk, paired,
    gain_hbm, g_hbm, u_hbm, d_hbm, x_hbm,
    wg, wu, wd, mixed,
    gain_row, stage_g, stage_u, stage_d, own_d, transit, normed, hidden, part, near, pair, far,
    in_gain, in_g, in_u, in_d, in_x, s_up, s_dn, s_y, s_det, r_w, s_one, s_tz, s_tx, r_t,
    s_dz, s_dy, r_d, s_a, r_a, s_b, r_b,
):
    f, t = lax.axis_index("fs"), lax.axis_index("tp")
    X = T // 2
    z, y = f // Y, lax.rem(f, Y)
    x, core = t // 2, lax.rem(t, 2)
    has_up, has_dn = z < Z - 1, z > 0
    up, dn = (f + Y, t), (f - Y, t)
    others = [lax.rem(y + i, Y) for i in range(1, Y)]
    across = [(z * Y + o, t) for o in others]
    rows = g_hbm.shape[0]
    ck = rows // nk
    rows_d, cols_d = d_hbm.shape
    pq = cols_d // W
    nc = T * pq
    n = x_hbm.shape[0]
    staged, full = (stage_g, stage_u), (wg, wu)
    pieces = [(k, a) for k in range(nk) for a in range(2)]

    def load(k, a):
        at = pl.ds(k * ck, ck)
        return pltpu.make_async_copy((g_hbm, u_hbm)[a].at[at, :], staged[a].at[at, :], (in_g, in_u)[a].at[k])

    load_d = pltpu.make_async_copy(d_hbm, stage_d, in_d.at[0])
    load_x = pltpu.make_async_copy(x_hbm, normed, in_x.at[0])
    load_gain = pltpu.make_async_copy(gain_hbm, gain_row, in_gain.at[0])
    load_gain.start()
    for k, a in pieces:
        load(k, a).start()
    load_d.start()
    load_x.start()

    barrier = pltpu.get_barrier_semaphore()

    def greet(dev):
        pl.semaphore_signal(barrier, inc=1, device_id=dev, device_id_type=MESH)

    when(has_up, lambda: greet(up))
    when(has_dn, lambda: greet(dn))
    for dev in across:
        greet(dev)
    for i in range(1, T):
        greet((f, lax.rem(t + i, T)))

    load_gain.wait()
    diagonal = lax.broadcasted_iota(jnp.int32, (rows, rows), 0) == lax.broadcasted_iota(jnp.int32, (rows, rows), 1)
    gain = jnp.sum(jnp.where(diagonal, jnp.broadcast_to(gain_row[...], (rows, rows)), 0.0), axis=1, keepdims=True)

    def copy(src, dst, ss, rs, dev):
        return pltpu.make_async_remote_copy(
            src_ref=src, dst_ref=dst, send_sem=ss, recv_sem=rs, device_id=dev, device_id_type=MESH
        )

    def weight(a, k, source, ss, dev):
        at = full[a].at[pl.ds(pl.multiple_of(source * rows + k * ck, ck), ck), :]
        return copy(at, at, ss, r_w.at[source, a, k], dev)

    def arrived(a, k, source):
        weight(a, k, source, s_det.at[0], (f, lax.rem(t + 1, T))).wait_recv()

    def start(cond, make):
        if cond is None:
            make().start()
        else:
            when(cond, lambda: make().start())

    def scale(k, a):
        load(k, a).wait()
        at = pl.ds(pl.multiple_of(f * rows + k * ck, ck), ck)
        full[a][at, :] = (gain[k * ck:(k + 1) * ck, :] * staged[a][pl.ds(k * ck, ck), :]).astype(jnp.bfloat16)

    def send_own(k, a):
        start(has_up, lambda: weight(a, k, f, s_up.at[z], up))
        start(has_dn, lambda: weight(a, k, f, s_dn.at[z], dn))
        for i in range(Y - 1):
            start(None, lambda i=i: weight(a, k, f, s_y.at[i, z], across[i]))

    scale(*pieces[0])
    scale(*pieces[1])
    pl.semaphore_wait(barrier, Y + T - 2 + has_up.astype(jnp.int32) + has_dn.astype(jnp.int32))
    for i, piece in enumerate(pieces):
        if i + 2 < len(pieces):
            scale(*pieces[i + 2])
        send_own(*piece)

    def cols(j):
        return pl.ds(pl.multiple_of(j * W, W), W)

    def line_rows(line):
        return pl.ds(pl.multiple_of(line * rows_d, rows_d), rows_d)

    def down(line, j, ss, dev):
        at = wd.at[line_rows(line), cols(j)]
        return copy(at, at, ss, r_d.at[line, j], dev)

    def down_arrived(line, j):
        down(line, j, s_dy.at[0, 0], (f, lax.rem(t + 1, T))).wait_recv()

    load_d.wait()
    own_d[...] = stage_d[...].astype(jnp.bfloat16)

    @pl.when(z == t)
    def _():
        wd[line_rows(y), pl.ds(pl.multiple_of(t * cols_d, cols_d), cols_d)] = stage_d[...].astype(jnp.bfloat16)

    def first(p):
        return copy(
            own_d.at[:, pl.ds(p * W, W)], wd.at[line_rows(y), cols(t * pq + p)],
            s_one.at[0], r_d.at[y, t * pq + p], (f, z),
        )

    load_x.wait()
    slab = 64 if n % 64 == 0 else n

    def normalise(i):
        at = pl.ds(pl.multiple_of(i * slab, slab), slab)
        v = normed[at, :].astype(jnp.float32)
        normed[at, :] = (v * lax.rsqrt(jnp.mean(v * v, axis=1, keepdims=True) + 1e-05)).astype(jnp.bfloat16)

    normalise(0)
    for p in range(pq):
        start(z != t, lambda p=p: first(p))
    each(1, n // slab, normalise)

    at_home = z == t
    can_up = jnp.logical_and(has_up, z >= t)
    can_dn = jnp.logical_and(has_dn, z <= t)
    inner = jnp.logical_and(has_up, has_dn)
    if paired:
        half = t // (T // 2)
        shift = (nc // 2) * (1 - half)
        far_up, far_dn = half == 0, half == 1
        beyond = jnp.logical_or(jnp.logical_and(z < t, far_dn), jnp.logical_and(z > t, far_up))
        fwd_mid = jnp.logical_or(
            jnp.logical_and(can_up, jnp.logical_not(far_up)), jnp.logical_and(can_dn, jnp.logical_not(far_dn))
        )
        mid_lo, mid_hi = 2 * pq, 2 * pq + pq // 2
    else:
        shift = 0
        mid_lo, mid_hi = 0, nc
    fwd_all = jnp.logical_or(can_up, can_dn)
    if paired:
        passes = jnp.logical_or(fwd_all, beyond)
    away = jnp.logical_not(at_home)

    def column(r):
        return lax.rem(r + shift, nc)

    def turned(r):
        return lax.rem(r + (nc // 2) * (z >= Z // 2).astype(jnp.int32), nc) if paired else r

    def pick(table, i):
        return turned(sum(p * (i == e).astype(jnp.int32) for e, p in enumerate(table)))

    pair_units, last_units = column_units(pq, nc, paired)
    sequence = [p + i for p in pair_units for i in range(2)] + list(last_units)

    def piece_of(i):
        return pick(sequence, i)

    bent = (pq if paired else 0, lambda i: column(core * pq + i), 0)
    low = (pq if paired else 0, lambda i: column((1 - core) * pq + i), 1)
    mid = (mid_hi - mid_lo, lambda i: column(mid_lo + i), 1)
    high = (nc - mid_hi, lambda i: column(mid_hi + i), 2)
    sizes = (bent[0], low[0] + mid[0], high[0])

    def over(kind, fn):
        each(0, kind[0], lambda i: fn(kind[1](i), kind[2]))

    def both(a, b):
        return jnp.logical_and(a, b)

    def kinds(j):
        r = lax.rem(j - shift + nc, nc)
        is_high = r >= mid_hi
        is_bent = both(r < 2 * pq, r // pq == core)
        return is_high, is_bent, jnp.logical_not(jnp.logical_or(is_high, is_bent))

    def z_send(line, j, kind, which, direction):
        return down(line, j, s_dz.at[direction, which, kind], (up, dn)[direction])

    def near_ok(direction):
        return jnp.logical_not((far_up, far_dn)[direction])

    def can(direction):
        return (can_up, can_dn)[direction]

    def cross(j, kind):
        for i in range(Y - 1):
            down(y, j, s_dy.at[i, kind], across[i]).start()

    other = others[0]

    def assemble():
        for i in range(1, T):
            owner = lax.rem(t + i, T)
            for p in range(pq):
                down_arrived(y, owner * pq + p)
        over(high, cross)
        if paired:
            @pl.when(inner)
            def _():
                over(low, cross)
                over(mid, cross)

    if paired:
        guest = lax.rem(t + T // 2, T)
        guest_dn = guest // (T // 2) == 1
        guest_here = jnp.logical_or(both(z < guest, guest_dn), both(z > guest, jnp.logical_not(guest_dn)))
        guest_on = (both(both(z >= guest, has_up), jnp.logical_not(guest_dn)), both(both(z <= guest, has_dn), guest_dn))

        def relay(p, direction, src):
            return copy(
                src.at[:, cols(p)], transit.at[:, cols(p)], s_tz.at[0], r_t.at[p], (up, dn)[direction]
            )

        def hand_over(p):
            return copy(
                transit.at[:, cols(p)], wd.at[line_rows(y), cols(t * pq + p)], s_tx.at[0], r_d.at[y, t * pq + p], (f, guest)
            )

    def leave(direction):
        if paired:
            @pl.when(both(z == guest, guest_on[direction]))
            def _():
                each(0, pq, lambda p: relay(p, direction, own_d).start())

        here = both(at_home, can(direction))
        if paired:
            here = both(here, jnp.logical_not(near_ok(direction)))

        @pl.when(here)
        def _():
            for kind in (low, mid, high):
                over(kind, lambda j, c: z_send(y, j, c, 0, direction).start())

    def hook(s):
        when(z == s, lambda: leave(0))
        when(z == Z - 1 - s, lambda: leave(1))

    for step in range(1, Z):
        for count, (k, a) in enumerate(pieces):
            if step == 1 and count == len(pieces) // 2:
                when(at_home, assemble)
            for sign in (-1, 1):
                zs = z + sign * step
                source = zs * Y + y
                valid = zs >= 0 if sign < 0 else zs < Z
                onward = jnp.logical_and(valid, has_up if sign < 0 else has_dn)
                when(valid, lambda a=a, k=k, s=source: arrived(a, k, s))
                if sign < 0:
                    start(onward, lambda a=a, k=k, s=source, q=zs: weight(a, k, s, s_up.at[q], up))
                else:
                    start(onward, lambda a=a, k=k, s=source, q=zs: weight(a, k, s, s_dn.at[q], dn))
                crossing = valid
                if paired and step == 1:
                    crossing = both(valid, zs != (0 if sign < 0 else Z - 1))
                for i in range(Y - 1):
                    start(crossing, lambda a=a, k=k, s=source, q=zs, i=i: weight(a, k, s, s_y.at[i, q], across[i]))
        if step == 1:
            hook(0)
            if paired:
                ends = jnp.logical_not(inner)
                beside = across[0][0]
                for k, a in pieces:
                    when(ends, lambda a=a, k=k: arrived(a, k, beside))
                    start(both(ends, has_up), lambda a=a, k=k: weight(a, k, beside, s_det.at[0], up))
                    start(both(ends, has_dn), lambda a=a, k=k: weight(a, k, beside, s_det.at[0], dn))
        hook(step)

    if paired:
        @pl.when(at_home)
        def _():
            @pl.when(jnp.logical_not(inner))
            def _():
                def late(i):
                    j = piece_of(i)
                    is_high, is_bent, is_mid = kinds(j)
                    when(jnp.logical_not(is_high), lambda: cross(j, is_mid.astype(jnp.int32)))
                each(0, nc, late)
            when(inner, lambda: over(bent, cross))

    else:
        when(at_home, lambda: over(mid, cross))

    if paired:
        @pl.when(guest_here)
        def _():
            def pass_on(p):
                copy(
                    transit.at[:, cols(p)], transit.at[:, cols(p)], s_tz.at[0], r_t.at[p], (f, guest)
                ).wait_recv()
                for direction in range(2):
                    when(guest_on[direction], lambda: relay(p, direction, transit).start())
                hand_over(p).start()
            each(0, pq, pass_on)

    if paired:
        @pl.when(both(at_home, inner))
        def _():
            def near_first(j, kind):
                for direction in range(2):
                    when(near_ok(direction), lambda: z_send(y, j, kind, 0, direction).start())
            over(bent, near_first)

            def near_pair(i):
                j = piece_of(i)
                is_high, is_bent, _ = kinds(j)
                kind = 1 + is_high.astype(jnp.int32)

                @pl.when(jnp.logical_not(is_bent))
                def _():
                    near_first(j, kind)
                    down_arrived(other, j)
                    for direction in range(2):
                        when(jnp.logical_or(near_ok(direction), is_high), lambda: z_send(other, j, kind, 1, direction).start())
            each(0, nc, near_pair)

    @pl.when(away)
    def _():
        def bend(j, kind):
            down_arrived(y, j)
            for direction in range(2):
                when(both(can(direction), near_ok(direction)), lambda: z_send(y, j, kind, 0, direction).start())
            cross(j, kind)

        def straight(j, kind):
            down_arrived(y, j)
            for direction in range(2):
                when(can(direction), lambda: z_send(y, j, kind, 0, direction).start())
            if paired:
                when(beyond, lambda: cross(j, kind))
            else:
                cross(j, kind)

        over(bent, bend)
        if paired:
            @pl.when(passes)
            def _():
                over(low, straight)
                over(mid, straight)
        else:
            over(mid, straight)

    if paired:
        @pl.when(both(fwd_mid, away))
        def _():
            def twin(j, kind):
                down_arrived(other, j)
                for direction in range(2):
                    when(both(can(direction), near_ok(direction)), lambda: z_send(other, j, kind, 1, direction).start())
            over(low, twin)
            over(mid, twin)

        @pl.when(both(fwd_all, jnp.logical_or(away, jnp.logical_not(inner))))
        def _():
            def twins(j, kind):
                @pl.when(away)
                def _():
                    down_arrived(y, j)
                    for direction in range(2):
                        when(can(direction), lambda: z_send(y, j, kind, 0, direction).start())
                down_arrived(other, j)
                for direction in range(2):
                    when(can(direction), lambda: z_send(other, j, kind, 1, direction).start())
            over(high, twins)

    for zs in range(Z):
        for o in others:
            for k, a in pieces:
                if paired and zs in (0, Z - 1):
                    when(zs != z, lambda a=a, k=k, zs=zs, o=o: arrived(a, k, zs * Y + o))
                else:
                    arrived(a, k, zs * Y + o)
    units = wg.shape[1]
    width = 256 if units % 256 == 0 else 128

    @pl.loop(0, units // width)
    def _(j):
        at = pl.ds(pl.multiple_of(j * width, width), width)
        gate = jnp.dot(normed[...], wg[:, at], preferred_element_type=jnp.float32)
        up_ = jnp.dot(normed[...], wu[:, at], preferred_element_type=jnp.float32)
        hidden[:, at] = (gate / (1.0 + jnp.exp(-gate)) * up_).astype(jnp.bfloat16)

    def drained(sem):
        both_shards = wg.at[pl.ds(0, 2 * rows), :]
        copy(both_shards, both_shards, sem, r_w.at[0, 0, 0], (f, lax.rem(t + 1, T))).wait_send()

    for q in range(Z):
        when(jnp.logical_and(has_up, q <= z), lambda q=q: drained(s_up.at[q]))
        when(jnp.logical_and(has_dn, q >= z), lambda q=q: drained(s_dn.at[q]))
        crossing = z >= 0
        if paired and q in (0, Z - 1):
            crossing = z != (1 if q == 0 else Z - 2)
        for i in range(Y - 1):
            when(crossing, lambda q=q, i=i: drained(s_y.at[i, q]))
    if paired:
        when(jnp.logical_not(inner), lambda: drained(s_det.at[0]))

    mate = (f, x * 2 + 1 - core)

    def span(j, count):
        return pl.ds(pl.multiple_of(j * W, W), count * W)

    def to_mate(j, count):
        return copy(part.at[:, span(j, count)], near.at[:, span(j, count)], s_a.at[0], r_a.at[j], mate)

    def to_owner(j, count, slot, dev):
        p = lax.rem(j, pq)
        return copy(pair.at[:, span(j, count)], far.at[slot, :, span(p, count)], s_b.at[0], r_b.at[slot, p], dev)

    def whole(j):
        if paired:
            is_high, is_bent, is_mid = kinds(j)
            late = both(is_high, jnp.logical_not(fwd_all))
            late_own = both(away, jnp.logical_or(late, both(is_mid, jnp.logical_not(passes))))
            when(late_own, lambda: down_arrived(y, j))
            late_other = jnp.logical_or(jnp.logical_or(late, is_bent), both(is_mid, jnp.logical_not(fwd_mid)))
            when(late_other, lambda: down_arrived(other, j))
        else:
            for o in others:
                down_arrived(o, j)

    def ours(j):
        return lax.rem(j // pq, 2) == core

    def abroad(j):
        return both(ours(j), j // pq // 2 != x)

    def products(table, count, lag):
        m = len(table)

        def multiply(j):
            for i in range(count):
                whole(j + i)
            at = span(j, count)
            part[:, at] = jnp.dot(hidden[...], wd[:, at], preferred_element_type=jnp.float32).astype(jnp.bfloat16)

        def add(j):
            at = span(j, count)
            when(ours(j), lambda: to_mate(j, count).wait_recv())

            @pl.when(abroad(j))
            def _():
                pair[:, at] = (part[:, at].astype(jnp.float32) + near[:, at].astype(jnp.float32)).astype(jnp.bfloat16)

        def ship(j):
            owner = j // pq
            to_owner(j, count, lax.rem(x - owner // 2 + X, X) - 1, (f, owner)).start()

        def step(i):
            now, then = i < m, i >= lag
            j0 = pick(table, jnp.minimum(i, m - 1))
            j1 = pick(table, jnp.maximum(i - lag, 0))
            if lag == 1:
                when(then, lambda: add(j1))
                when(both(then, abroad(j1)), lambda: ship(j1))
                when(now, lambda: multiply(j0))
                when(both(now, jnp.logical_not(ours(j0))), lambda: to_mate(j0, count).start())
            else:
                when(now, lambda: multiply(j0))
                when(then, lambda: add(j1))
                when(both(now, jnp.logical_not(ours(j0))), lambda: to_mate(j0, count).start())
                when(both(then, abroad(j1)), lambda: ship(j1))

        each(0, m + lag, step)

    def finish(table, count):
        def step(i):
            j = pick(table, i)

            @pl.when(j // pq == t)
            def _():
                at, to = span(j, count), span(lax.rem(j, pq), count)
                acc = part[:, at].astype(jnp.float32) + near[:, at].astype(jnp.float32)
                for slot in range(X - 1):
                    to_owner(j, count, slot, mate).wait_recv()
                    acc = acc + far[slot, :, to].astype(jnp.float32)
                mixed[:, to] = acc.astype(mixed.dtype)

        each(0, len(table), step)

    if pair_units:
        products(pair_units, 2, 2)
    products(last_units, 1, 1)
    if pair_units:
        finish(pair_units, 2)

    def gone(sem, ref):
        copy(ref, ref, sem, r_a.at[0], mate).wait_send()

    def gone_down(sem, kind):
        if sizes[kind]:
            gone(sem, wd.at[pl.ds(0, rows_d), pl.ds(0, sizes[kind] * W)])

    when(away, lambda: gone(s_one.at[0], own_d))
    if paired:
        when(jnp.logical_or(guest_on[0], guest_on[1]), lambda: gone(s_tz.at[0], transit))
        when(guest_here, lambda: gone(s_tx.at[0], transit))
    for direction in range(2):
        if paired:
            near_dir = both(can(direction), near_ok(direction))
            when(near_dir, lambda: gone_down(s_dz.at[direction, 0, 0], 0))
            when(near_dir, lambda: gone_down(s_dz.at[direction, 1, 1], 1))
            when(can(direction), lambda: gone_down(s_dz.at[direction, 0, 2], 2))
            when(can(direction), lambda: gone_down(s_dz.at[direction, 1, 2], 2))
        when(can(direction), lambda: gone_down(s_dz.at[direction, 0, 1], 1))
    for i in range(Y - 1):
        if paired:
            gone_down(s_dy.at[i, 0], 0)
            when(jnp.logical_or(at_home, beyond), lambda: gone_down(s_dy.at[i, 1], 1))
            when(at_home, lambda: gone_down(s_dy.at[i, 2], 2))
        else:
            gone_down(s_dy.at[i, 1], 1)
    finish(last_units, 1)
    gone(s_a.at[0], part.at[:, pl.ds(0, nc * W // 2)])
    gone(s_b.at[0], pair.at[:, pl.ds(0, (X - 1) * pq * W)])


def layer(mesh, gain, g, u, d, x):
    fs, T = mesh.shape["fs"], mesh.shape["tp"]
    Z, Y = lines(fs)
    X = T // 2
    rows, rows_d, n = g.shape[0], d.shape[0], x.shape[0]
    pq = d.shape[1] // W
    nc = T * pq
    nk = max(1, min(4, rows // 64))
    paired = Y == 2 and X == 2 and Z == T and pq % 2 == 0
    lanes = max(Y - 1, 1)
    dma = pltpu.SemaphoreType.DMA
    vmem, hbm = pl.BlockSpec(memory_space=pltpu.VMEM), pl.BlockSpec(memory_space=pltpu.HBM)
    bf = jnp.bfloat16
    return pl.pallas_call(
        functools.partial(layer_kernel, Z, Y, T, nk, paired),
        out_shape=(
            jax.ShapeDtypeStruct((rows * fs, g.shape[1]), bf),
            jax.ShapeDtypeStruct((rows * fs, g.shape[1]), bf),
            jax.ShapeDtypeStruct((rows_d * Y, d.shape[1] * T), bf),
            jax.ShapeDtypeStruct((n, d.shape[1]), bf),
        ),
        in_specs=[hbm] * 5,
        out_specs=[vmem] * 4,
        scratch_shapes=[
            pltpu.VMEM(gain.shape, jnp.float32),
            pltpu.VMEM(g.shape, jnp.float32), pltpu.VMEM(u.shape, jnp.float32), pltpu.VMEM(d.shape, jnp.float32),
            pltpu.VMEM(d.shape, bf), pltpu.VMEM(d.shape, bf), pltpu.VMEM(x.shape, bf), pltpu.VMEM((n, g.shape[1]), bf),
            pltpu.VMEM((n, nc * W), bf), pltpu.VMEM((n, nc * W), bf), pltpu.VMEM((n, nc * W), bf),
            pltpu.VMEM((max(X - 1, 1), n, pq * W), bf),
            dma((1,)), dma((nk,)), dma((nk,)), dma((1,)), dma((1,)),
            dma((Z,)), dma((Z,)), dma((lanes, Z)), dma((1,)), dma((fs, 2, nk)),
            dma((1,)), dma((1,)), dma((1,)), dma((pq,)),
            dma((2, 2, 3)), dma((lanes, 3)), dma((Y, nc)),
            dma((1,)), dma((nc,)), dma((1,)), dma((max(X - 1, 1), pq)),
        ],
        compiler_params=pltpu.CompilerParams(
            collective_id=0, has_side_effects=True, vmem_limit_bytes=GRANT
        ),
        name="layer",
    )(*(pltpu.with_memory_space_constraint(v, pltpu.HBM) for v in (gain, g, u, d, x)))


def publish_kernel(cuts, wg, wu, wd, mixed, og, ou, od, om, sems):
    outs = []
    for a, (s, d) in enumerate(((wg, og), (wu, ou), (wd, od), (mixed, om))):
        h = s.shape[0] // cuts
        for i in range(cuts):
            outs.append(pltpu.make_async_copy(s.at[pl.ds(i * h, h), :], d.at[pl.ds(i * h, h), :], sems.at[a, i]))
    for c in outs:
        c.start()
    for c in outs:
        c.wait()


def publish(*arrays):
    vmem, any_ = pl.BlockSpec(memory_space=pltpu.VMEM), pl.BlockSpec(memory_space=pl.ANY)
    return pl.pallas_call(
        functools.partial(publish_kernel, CUTS),
        out_shape=tuple(jax.ShapeDtypeStruct(a.shape, a.dtype) for a in arrays),
        in_specs=[vmem] * 4,
        out_specs=[any_] * 4,
        scratch_shapes=[pltpu.SemaphoreType.DMA((4, CUTS))],
        compiler_params=pltpu.CompilerParams(vmem_limit_bytes=1024 * 1024),
        name="publish",
    )(*arrays)


def solution(mesh):
    def on_device(tokens, norm_gain, gate_weight, up_weight, down_weight):
        wg, wu, wd, mixed = layer(mesh, norm_gain[None, :], gate_weight, up_weight, down_weight, tokens)
        og, ou, od, om = publish(wg, wu, wd, mixed)
        return (om, og, ou, od)

    return jax.shard_map(
        on_device,
        mesh=mesh,
        in_specs=(P("fs", None), P("fs"), P("fs", "tp"), P("fs", "tp"), P("fs", "tp")),
        out_specs=(P("fs", "tp"), P(None, "tp"), P(None, "tp"), P("tp", None)),
        check_vma=False,
    )
```

time: 217 us -> 197 us (0.908)
  Pallas kernels: 214 us -> 195 us
    pallas_call x1, Pallas kernels: 207 us -> 188 us  [layer(): pl.pallas_call(functools.partial(layer_kernel, Z, Y, T, nk, paired), out_...]
where the time goes in v2:
time: 197 us; the launch traced here: 196 us
  Pallas kernels  195 us (99%)
    pallas_call x1, Pallas kernels, layer(): pl.pallas_call(functools.partial(layer_kernel, Z, Y, T, nk, paired), out_...  188 us
    pallas_call x1, Pallas kernels, publish(): pl.pallas_call(functools.partial(publish_kernel, CUTS), out_shape=tuple((...  6.73 us

profile of v2, /device:TPU:0, one launch (start us, length us, event | category | flops | bytes accessed | tf_op | source)
XLA Modules:
  0.0 195.6 jit_solution(14447419658156184991)
XLA Ops:
  0.6 188.2 %layer.1 = (bf16[2048,1536]{1,0:T(8,128)(2,1)S(1)}, bf16[2048,1536]{1,0:T(8,128)(2,1)S(1)}, bf16[1536,2048]{1,0:T(8,128)(2,1)S(1)}, bf16[512,512]{1,0:T(8,128)(2,1)S(1)}) custom-call(f32[1,256]{1,0:T(1,128)} %bitcast.1, f32[256,1536]{1,0:T(8,128)} %g_hbm.1, f32[256,1536]{1,0:T(8,128)} %u_hbm.1, f32[768,512]{1,0:T(8,128)} %d_hbm.1, bf16[512,2048]{1,0:T(8,128)(2,1)} %x_hbm.1), custom_call_target="tpu_custom_call" | custom-call | tf_op jit(solution)/shard_map/layer/pallas_call | solution.py:588
  188.8 6.7 %publish.1 = (bf16[2048,1536]{1,0:T(8,128)(2,1)}, bf16[2048,1536]{1,0:T(8,128)(2,1)}, bf16[1536,2048]{1,0:T(8,128)(2,1)}, bf16[512,512]{1,0:T(8,128)(2,1)}) custom-call(bf16[2048,1536]{1,0:T(8,128)(2,1)S(1)} %get-tuple-element.12.wg, bf16[2048,1536]{1,0:T(8,128)(2,1)S(1)} %get-tuple-element.13.wu, bf16[1536,2048]{1,0:T(8,128)(2,1)S(1)} %get-tuple-element.14.wd, ...), custom_call_target="tpu_custom_call" | custom-call | tf_op jit(solution)/shard_map/publish/pallas_call | solution.py:631

commit v3 on v2

--- a/solution.py
+++ b/solution.py
@@ -44,7 +44,7 @@
         return (), tuple(sorted(range(nc), key=lambda p: times[p]))
     pairs = sorted(range(0, nc, 2), key=lambda p: max(times[p], times[p + 1]))
     ends = [p + i for p in pairs[-2:] for i in range(2)]
-    return tuple(pairs[:-2]), tuple(sorted(ends, key=lambda p: times[p]))
+    return tuple(pairs[:-2]), tuple(sorted(ends, key=lambda p: (times[p], -p)))
 
 
 def layer_kernel(
@@ -52,8 +52,8 @@
     gain_hbm, g_hbm, u_hbm, d_hbm, x_hbm,
     wg, wu, wd, mixed,
     gain_row, stage_g, stage_u, stage_d, own_d, transit, normed, hidden, part, near, pair, far,
-    in_gain, in_g, in_u, in_d, in_x, s_up, s_dn, s_y, s_det, r_w, s_one, s_tz, s_tx, r_t,
-    s_dz, s_dy, r_d, s_a, r_a, s_b, r_b,
+    in_gain, in_g, in_u, in_d, in_x, s_up, s_dn, s_y, s_det, r_w, r_o, s_one, s_tz, s_tx, r_t,
+    s_dz, s_dy, r_d, s_a, r_a, s_b, r_b, r_c,
 ):
     f, t = lax.axis_index("fs"), lax.axis_index("tp")
     X = T // 2
@@ -106,12 +106,25 @@
             src_ref=src, dst_ref=dst, send_sem=ss, recv_sem=rs, device_id=dev, device_id_type=MESH
         )
 
-    def weight(a, k, source, ss, dev):
+    def weight(a, k, source, ss, rs, dev):
         at = full[a].at[pl.ds(pl.multiple_of(source * rows + k * ck, ck), ck), :]
-        return copy(at, at, ss, r_w.at[source, a, k], dev)
-
-    def arrived(a, k, source):
-        weight(a, k, source, s_det.at[0], (f, lax.rem(t + 1, T))).wait_recv()
+        return copy(at, at, ss, rs, dev)
+
+    def along(a, k, source, ss, dev):
+        return weight(a, k, source, ss, r_w.at[source // Y, k], dev)
+
+    def beyond_line(a, k, source, ss, dev):
+        return weight(a, k, source, ss, r_o.at[source], dev)
+
+    def taken(height, ss, rs):
+        at = wg.at[pl.ds(0, height), :]
+        return copy(at, at, ss, rs, (f, lax.rem(t + 1, T)))
+
+    def arrived(k, source):
+        taken(2 * ck, s_det.at[0], r_w.at[source // Y, k]).wait_recv()
+
+    def arrived_whole(source):
+        taken(2 * rows, s_det.at[0], r_o.at[source]).wait_recv()
 
     def start(cond, make):
         if cond is None:
@@ -125,10 +138,10 @@
         full[a][at, :] = (gain[k * ck:(k + 1) * ck, :] * staged[a][pl.ds(k * ck, ck), :]).astype(jnp.bfloat16)
 
     def send_own(k, a):
-        start(has_up, lambda: weight(a, k, f, s_up.at[z], up))
-        start(has_dn, lambda: weight(a, k, f, s_dn.at[z], dn))
+        start(has_up, lambda: along(a, k, f, s_up.at[0], up))
+        start(has_dn, lambda: along(a, k, f, s_dn.at[0], dn))
         for i in range(Y - 1):
-            start(None, lambda i=i: weight(a, k, f, s_y.at[i, z], across[i]))
+            start(None, lambda i=i: beyond_line(a, k, f, s_y.at[i], across[i]))
 
     scale(*pieces[0])
     scale(*pieces[1])
@@ -149,7 +162,7 @@
         return copy(at, at, ss, r_d.at[line, j], dev)
 
     def down_arrived(line, j):
-        down(line, j, s_dy.at[0, 0], (f, lax.rem(t + 1, T))).wait_recv()
+        down(line, j, s_dy.at[0], (f, lax.rem(t + 1, T))).wait_recv()
 
     load_d.wait()
     own_d[...] = stage_d[...].astype(jnp.bfloat16)
@@ -213,14 +226,13 @@
     def piece_of(i):
         return pick(sequence, i)
 
-    bent = (pq if paired else 0, lambda i: column(core * pq + i), 0)
-    low = (pq if paired else 0, lambda i: column((1 - core) * pq + i), 1)
-    mid = (mid_hi - mid_lo, lambda i: column(mid_lo + i), 1)
-    high = (nc - mid_hi, lambda i: column(mid_hi + i), 2)
-    sizes = (bent[0], low[0] + mid[0], high[0])
+    bent = (pq if paired else 0, lambda i: column(core * pq + i))
+    low = (pq if paired else 0, lambda i: column((1 - core) * pq + i))
+    mid = (mid_hi - mid_lo, lambda i: column(mid_lo + i))
+    high = (nc - mid_hi, lambda i: column(mid_hi + i))
 
     def over(kind, fn):
-        each(0, kind[0], lambda i: fn(kind[1](i), kind[2]))
+        each(0, kind[0], lambda i: fn(kind[1](i)))
 
     def both(a, b):
         return jnp.logical_and(a, b)
@@ -231,8 +243,8 @@
         is_bent = both(r < 2 * pq, r // pq == core)
         return is_high, is_bent, jnp.logical_not(jnp.logical_or(is_high, is_bent))
 
-    def z_send(line, j, kind, which, direction):
-        return down(line, j, s_dz.at[direction, which, kind], (up, dn)[direction])
+    def z_send(line, j, direction):
+        return down(line, j, s_dz.at[direction], (up, dn)[direction])
 
     def near_ok(direction):
         return jnp.logical_not((far_up, far_dn)[direction])
@@ -240,9 +252,9 @@
     def can(direction):
         return (can_up, can_dn)[direction]
 
-    def cross(j, kind):
+    def cross(j):
         for i in range(Y - 1):
-            down(y, j, s_dy.at[i, kind], across[i]).start()
+            down(y, j, s_dy.at[i], across[i]).start()
 
     other = others[0]
 
@@ -287,40 +299,41 @@
         @pl.when(here)
         def _():
             for kind in (low, mid, high):
-                over(kind, lambda j, c: z_send(y, j, c, 0, direction).start())
+                over(kind, lambda j: z_send(y, j, direction).start())
 
     def hook(s):
         when(z == s, lambda: leave(0))
         when(z == Z - 1 - s, lambda: leave(1))
 
     for step in range(1, Z):
-        for count, (k, a) in enumerate(pieces):
-            if step == 1 and count == len(pieces) // 2:
+        for k in range(nk):
+            if step == 1 and k == nk // 2:
                 when(at_home, assemble)
             for sign in (-1, 1):
                 zs = z + sign * step
                 source = zs * Y + y
                 valid = zs >= 0 if sign < 0 else zs < Z
                 onward = jnp.logical_and(valid, has_up if sign < 0 else has_dn)
-                when(valid, lambda a=a, k=k, s=source: arrived(a, k, s))
-                if sign < 0:
-                    start(onward, lambda a=a, k=k, s=source, q=zs: weight(a, k, s, s_up.at[q], up))
-                else:
-                    start(onward, lambda a=a, k=k, s=source, q=zs: weight(a, k, s, s_dn.at[q], dn))
                 crossing = valid
                 if paired and step == 1:
                     crossing = both(valid, zs != (0 if sign < 0 else Z - 1))
-                for i in range(Y - 1):
-                    start(crossing, lambda a=a, k=k, s=source, q=zs, i=i: weight(a, k, s, s_y.at[i, q], across[i]))
+                when(valid, lambda k=k, s=source: arrived(k, s))
+                for a in range(2):
+                    if sign < 0:
+                        start(onward, lambda a=a, k=k, s=source: along(a, k, s, s_up.at[0], up))
+                    else:
+                        start(onward, lambda a=a, k=k, s=source: along(a, k, s, s_dn.at[0], dn))
+                    for i in range(Y - 1):
+                        start(crossing, lambda a=a, k=k, s=source, i=i: beyond_line(a, k, s, s_y.at[i], across[i]))
         if step == 1:
             hook(0)
             if paired:
                 ends = jnp.logical_not(inner)
                 beside = across[0][0]
+                when(ends, lambda: arrived_whole(beside))
                 for k, a in pieces:
-                    when(ends, lambda a=a, k=k: arrived(a, k, beside))
-                    start(both(ends, has_up), lambda a=a, k=k: weight(a, k, beside, s_det.at[0], up))
-                    start(both(ends, has_dn), lambda a=a, k=k: weight(a, k, beside, s_det.at[0], dn))
+                    start(both(ends, has_up), lambda a=a, k=k: beyond_line(a, k, beside, s_det.at[0], up))
+                    start(both(ends, has_dn), lambda a=a, k=k: beyond_line(a, k, beside, s_det.at[0], dn))
         hook(step)
 
     if paired:
@@ -330,8 +343,8 @@
             def _():
                 def late(i):
                     j = piece_of(i)
-                    is_high, is_bent, is_mid = kinds(j)
-                    when(jnp.logical_not(is_high), lambda: cross(j, is_mid.astype(jnp.int32)))
+                    is_high, _, _ = kinds(j)
+                    when(jnp.logical_not(is_high), lambda: cross(j))
                 each(0, nc, late)
             when(inner, lambda: over(bent, cross))
 
@@ -353,40 +366,39 @@
     if paired:
         @pl.when(both(at_home, inner))
         def _():
-            def near_first(j, kind):
+            def near_first(j):
                 for direction in range(2):
-                    when(near_ok(direction), lambda: z_send(y, j, kind, 0, direction).start())
+                    when(near_ok(direction), lambda: z_send(y, j, direction).start())
             over(bent, near_first)
 
             def near_pair(i):
                 j = piece_of(i)
                 is_high, is_bent, _ = kinds(j)
-                kind = 1 + is_high.astype(jnp.int32)
 
                 @pl.when(jnp.logical_not(is_bent))
                 def _():
-                    near_first(j, kind)
+                    near_first(j)
                     down_arrived(other, j)
                     for direction in range(2):
-                        when(jnp.logical_or(near_ok(direction), is_high), lambda: z_send(other, j, kind, 1, direction).start())
+                        when(jnp.logical_or(near_ok(direction), is_high), lambda: z_send(other, j, direction).start())
             each(0, nc, near_pair)
 
     @pl.when(away)
     def _():
-        def bend(j, kind):
+        def bend(j):
             down_arrived(y, j)
             for direction in range(2):
-                when(both(can(direction), near_ok(direction)), lambda: z_send(y, j, kind, 0, direction).start())
-            cross(j, kind)
-
-        def straight(j, kind):
+                when(both(can(direction), near_ok(direction)), lambda: z_send(y, j, direction).start())
+            cross(j)
+
+        def straight(j):
             down_arrived(y, j)
             for direction in range(2):
-                when(can(direction), lambda: z_send(y, j, kind, 0, direction).start())
+                when(can(direction), lambda: z_send(y, j, direction).start())
             if paired:
-                when(beyond, lambda: cross(j, kind))
+                when(beyond, lambda: cross(j))
             else:
-                cross(j, kind)
+                cross(j)
 
         over(bent, bend)
         if paired:
@@ -400,33 +412,32 @@
     if paired:
         @pl.when(both(fwd_mid, away))
         def _():
-            def twin(j, kind):
+            def twin(j):
                 down_arrived(other, j)
                 for direction in range(2):
-                    when(both(can(direction), near_ok(direction)), lambda: z_send(other, j, kind, 1, direction).start())
+                    when(both(can(direction), near_ok(direction)), lambda: z_send(other, j, direction).start())
             over(low, twin)
             over(mid, twin)
 
         @pl.when(both(fwd_all, jnp.logical_or(away, jnp.logical_not(inner))))
         def _():
-            def twins(j, kind):
+            def twins(j):
                 @pl.when(away)
                 def _():
                     down_arrived(y, j)
                     for direction in range(2):
-                        when(can(direction), lambda: z_send(y, j, kind, 0, direction).start())
+                        when(can(direction), lambda: z_send(y, j, direction).start())
                 down_arrived(other, j)
                 for direction in range(2):
-                    when(can(direction), lambda: z_send(other, j, kind, 1, direction).start())
+                    when(can(direction), lambda: z_send(other, j, direction).start())
             over(high, twins)
 
     for zs in range(Z):
         for o in others:
-            for k, a in pieces:
-                if paired and zs in (0, Z - 1):
-                    when(zs != z, lambda a=a, k=k, zs=zs, o=o: arrived(a, k, zs * Y + o))
-                else:
-                    arrived(a, k, zs * Y + o)
+            if paired and zs in (0, Z - 1):
+                when(zs != z, lambda zs=zs, o=o: arrived_whole(zs * Y + o))
+            else:
+                arrived_whole(zs * Y + o)
     units = wg.shape[1]
     width = 256 if units % 256 == 0 else 128
 
@@ -437,32 +448,39 @@
         up_ = jnp.dot(normed[...], wu[:, at], preferred_element_type=jnp.float32)
         hidden[:, at] = (gate / (1.0 + jnp.exp(-gate)) * up_).astype(jnp.bfloat16)
 
-    def drained(sem):
-        both_shards = wg.at[pl.ds(0, 2 * rows), :]
-        copy(both_shards, both_shards, sem, r_w.at[0, 0, 0], (f, lax.rem(t + 1, T))).wait_send()
-
-    for q in range(Z):
-        when(jnp.logical_and(has_up, q <= z), lambda q=q: drained(s_up.at[q]))
-        when(jnp.logical_and(has_dn, q >= z), lambda q=q: drained(s_dn.at[q]))
-        crossing = z >= 0
-        if paired and q in (0, Z - 1):
-            crossing = z != (1 if q == 0 else Z - 2)
-        for i in range(Y - 1):
-            when(crossing, lambda q=q, i=i: drained(s_y.at[i, q]))
-    if paired:
-        when(jnp.logical_not(inner), lambda: drained(s_det.at[0]))
+    def drained(cond, shards, sem):
+        when(cond, lambda: taken(2 * rows * shards, sem, r_w.at[0, 0]).wait_send())
+
+    for q in range(Z - 1):
+        drained(z == q, q + 1, s_up.at[0])
+        drained(z == Z - 1 - q, q + 1, s_dn.at[0])
+    for i in range(Y - 1):
+        if paired:
+            drained(inner, Z - 1, s_y.at[i])
+            drained(jnp.logical_not(inner), Z, s_y.at[i])
+        else:
+            drained(z >= 0, Z, s_y.at[i])
+    if paired:
+        drained(jnp.logical_not(inner), 1, s_det.at[0])
 
     mate = (f, x * 2 + 1 - core)
 
     def span(j, count):
         return pl.ds(pl.multiple_of(j * W, W), count * W)
 
-    def to_mate(j, count):
-        return copy(part.at[:, span(j, count)], near.at[:, span(j, count)], s_a.at[0], r_a.at[j], mate)
-
-    def to_owner(j, count, slot, dev):
-        p = lax.rem(j, pq)
-        return copy(pair.at[:, span(j, count)], far.at[slot, :, span(p, count)], s_b.at[0], r_b.at[slot, p], dev)
+    def height(half, halves):
+        return pl.ds(pl.multiple_of(half * (n // halves), n // halves), n // halves)
+
+    def to_mate(j, count, half, halves, unit):
+        at = (height(half, halves), span(j, count))
+        return copy(part.at[at], near.at[at], s_a.at[0], r_a.at[unit], mate)
+
+    def to_owner(j, count, half, halves, slot, rs, dev):
+        h, p = height(half, halves), lax.rem(j, pq)
+        return copy(pair.at[h, span(j, count)], far.at[slot, h, span(p, count)], s_b.at[0], rs, dev)
+
+    def owner_sem(j, half, halves, slot):
+        return r_b.at[slot, lax.rem(j, pq)] if halves == 1 else r_c.at[slot, lax.rem(j, pq) * halves + half]
 
     def whole(j):
         if paired:
@@ -482,92 +500,101 @@
     def abroad(j):
         return both(ours(j), j // pq // 2 != x)
 
-    def products(table, count, lag):
-        m = len(table)
-
-        def multiply(j):
-            for i in range(count):
-                whole(j + i)
-            at = span(j, count)
-            part[:, at] = jnp.dot(hidden[...], wd[:, at], preferred_element_type=jnp.float32).astype(jnp.bfloat16)
-
-        def add(j):
-            at = span(j, count)
-            when(ours(j), lambda: to_mate(j, count).wait_recv())
+    def products(table, count, halves, lag, base):
+        m = len(table) * halves
+
+        def multiply(j, half):
+            def wait():
+                for i in range(count):
+                    whole(j + i)
+
+            when(half == 0, wait)
+            h, at = height(half, halves), span(j, count)
+            part[h, at] = jnp.dot(hidden[h, :], wd[:, at], preferred_element_type=jnp.float32).astype(jnp.bfloat16)
+
+        def add(j, half, unit):
+            h, at = height(half, halves), span(j, count)
+            when(ours(j), lambda: to_mate(j, count, half, halves, unit).wait_recv())
 
             @pl.when(abroad(j))
             def _():
-                pair[:, at] = (part[:, at].astype(jnp.float32) + near[:, at].astype(jnp.float32)).astype(jnp.bfloat16)
-
-        def ship(j):
+                pair[h, at] = (part[h, at].astype(jnp.float32) + near[h, at].astype(jnp.float32)).astype(jnp.bfloat16)
+
+        def ship(j, half):
             owner = j // pq
-            to_owner(j, count, lax.rem(x - owner // 2 + X, X) - 1, (f, owner)).start()
+            slot = lax.rem(x - owner // 2 + X, X) - 1
+            to_owner(j, count, half, halves, slot, owner_sem(j, half, halves, slot), (f, owner)).start()
 
         def step(i):
             now, then = i < m, i >= lag
-            j0 = pick(table, jnp.minimum(i, m - 1))
-            j1 = pick(table, jnp.maximum(i - lag, 0))
+            i0, i1 = jnp.minimum(i, m - 1), jnp.maximum(i - lag, 0)
+            j0, j1 = pick(table, i0 // halves), pick(table, i1 // halves)
+            h0, h1 = lax.rem(i0, halves), lax.rem(i1, halves)
+
+            def first_half():
+                when(now, lambda: multiply(j0, h0))
+                when(both(now, jnp.logical_not(ours(j0))), lambda: to_mate(j0, count, h0, halves, base + i).start())
+
+            def second_half():
+                when(then, lambda: add(j1, h1, base + i - lag))
+                when(both(then, abroad(j1)), lambda: ship(j1, h1))
+
             if lag == 1:
-                when(then, lambda: add(j1))
-                when(both(then, abroad(j1)), lambda: ship(j1))
-                when(now, lambda: multiply(j0))
-                when(both(now, jnp.logical_not(ours(j0))), lambda: to_mate(j0, count).start())
+                second_half()
+                first_half()
             else:
-                when(now, lambda: multiply(j0))
-                when(then, lambda: add(j1))
-                when(both(now, jnp.logical_not(ours(j0))), lambda: to_mate(j0, count).start())
-                when(both(then, abroad(j1)), lambda: ship(j1))
-
-        each(0, m + lag, step)
-
-    def finish(table, count):
+                first_half()
+                second_half()
+
+        each(0, m + lag if m else 0, step)
+
+    def finish(table, count, halves):
         def step(i):
-            j = pick(table, i)
+            j, half = pick(table, i // halves), lax.rem(i, halves)
 
             @pl.when(j // pq == t)
             def _():
-                at, to = span(j, count), span(lax.rem(j, pq), count)
-                acc = part[:, at].astype(jnp.float32) + near[:, at].astype(jnp.float32)
+                h, at, to = height(half, halves), span(j, count), span(lax.rem(j, pq), count)
+                acc = part[h, at].astype(jnp.float32) + near[h, at].astype(jnp.float32)
                 for slot in range(X - 1):
-                    to_owner(j, count, slot, mate).wait_recv()
-                    acc = acc + far[slot, :, to].astype(jnp.float32)
-                mixed[:, to] = acc.astype(mixed.dtype)
-
-        each(0, len(table), step)
-
-    if pair_units:
-        products(pair_units, 2, 2)
-    products(last_units, 1, 1)
-    if pair_units:
-        finish(pair_units, 2)
+                    to_owner(j, count, half, halves, slot, owner_sem(j, half, halves, slot), mate).wait_recv()
+                    acc = acc + far[slot, h, to].astype(jnp.float32)
+                mixed[h, to] = acc.astype(mixed.dtype)
+
+        each(0, len(table) * halves, step)
+
+    early, late_units = last_units[:-2], last_units[-2:]
+    halves = 2 if n % 32 == 0 else 1
+    products(pair_units, 2, 1, 2, 0)
+    products(early, 1, 1, 1, len(pair_units))
+    products(late_units, 1, halves, 2, len(pair_units) + len(early))
+    finish(pair_units, 2, 1)
+    finish(early, 1, 1)
 
     def gone(sem, ref):
         copy(ref, ref, sem, r_a.at[0], mate).wait_send()
 
-    def gone_down(sem, kind):
-        if sizes[kind]:
-            gone(sem, wd.at[pl.ds(0, rows_d), pl.ds(0, sizes[kind] * W)])
+    def gone_down(cond, sem, count):
+        fold = next(c for c in range(1, Y + 1) if count % c == 0 and count // c <= nc)
+        when(cond, lambda: gone(sem, wd.at[pl.ds(0, fold * rows_d), pl.ds(0, count // fold * W)]))
 
     when(away, lambda: gone(s_one.at[0], own_d))
     if paired:
         when(jnp.logical_or(guest_on[0], guest_on[1]), lambda: gone(s_tz.at[0], transit))
         when(guest_here, lambda: gone(s_tx.at[0], transit))
-    for direction in range(2):
-        if paired:
-            near_dir = both(can(direction), near_ok(direction))
-            when(near_dir, lambda: gone_down(s_dz.at[direction, 0, 0], 0))
-            when(near_dir, lambda: gone_down(s_dz.at[direction, 1, 1], 1))
-            when(can(direction), lambda: gone_down(s_dz.at[direction, 0, 2], 2))
-            when(can(direction), lambda: gone_down(s_dz.at[direction, 1, 2], 2))
-        when(can(direction), lambda: gone_down(s_dz.at[direction, 0, 1], 1))
-    for i in range(Y - 1):
-        if paired:
-            gone_down(s_dy.at[i, 0], 0)
-            when(jnp.logical_or(at_home, beyond), lambda: gone_down(s_dy.at[i, 1], 1))
-            when(at_home, lambda: gone_down(s_dy.at[i, 2], 2))
-        else:
-            gone_down(s_dy.at[i, 1], 1)
-    finish(last_units, 1)
+        for direction in range(2):
+            gone_down(both(can(direction), near_ok(direction)), s_dz.at[direction], 2 * nc - pq)
+            on = both(can(direction), jnp.logical_not(near_ok(direction)))
+            gone_down(on, s_dz.at[direction], nc - pq + high[0])
+        gone_down(at_home, s_dy.at[0], nc)
+        gone_down(beyond, s_dy.at[0], nc - high[0])
+        gone_down(both(away, jnp.logical_not(beyond)), s_dy.at[0], pq)
+    else:
+        for direction in range(2):
+            gone_down(can(direction), s_dz.at[direction], nc)
+        for i in range(Y - 1):
+            gone_down(z >= 0, s_dy.at[i], nc)
+    finish(late_units, 1, halves)
     gone(s_a.at[0], part.at[:, pl.ds(0, nc * W // 2)])
     gone(s_b.at[0], pair.at[:, pl.ds(0, (X - 1) * pq * W)])
 
@@ -602,10 +629,11 @@
             pltpu.VMEM((n, nc * W), bf), pltpu.VMEM((n, nc * W), bf), pltpu.VMEM((n, nc * W), bf),
             pltpu.VMEM((max(X - 1, 1), n, pq * W), bf),
             dma((1,)), dma((nk,)), dma((nk,)), dma((1,)), dma((1,)),
-            dma((Z,)), dma((Z,)), dma((lanes, Z)), dma((1,)), dma((fs, 2, nk)),
+            dma((1,)), dma((1,)), dma((lanes,)), dma((1,)), dma((Z, nk)), dma((fs,)),
             dma((1,)), dma((1,)), dma((1,)), dma((pq,)),
-            dma((2, 2, 3)), dma((lanes, 3)), dma((Y, nc)),
-            dma((1,)), dma((nc,)), dma((1,)), dma((max(X - 1, 1), pq)),
+            dma((2,)), dma((lanes,)), dma((Y, nc)),
+            dma((1,)), dma((sum(map(len, column_units(pq, nc, paired))) + 2,)), dma((1,)), dma((max(X - 1, 1), pq)),
+            dma((max(X - 1, 1), 2 * pq)),
         ],
         compiler_params=pltpu.CompilerParams(
             collective_id=0, has_side_effects=True, vmem_limit_bytes=GRANT

time: 197 us -> 195 us (0.990)
  no operation moved by 1% of the time
where the time goes in v3:
time: 195 us
  Pallas kernels  194 us (99%)
    pallas_call x1, Pallas kernels, layer(): pl.pallas_call(functools.partial(layer_kernel, Z, Y, T, nk, paired), out_...  187 us
    pallas_call x1, Pallas kernels, publish(): pl.pallas_call(functools.partial(publish_kernel, CUTS), out_shape=tuple((...  6.73 us

profile of v3, /device:TPU:0, one launch (start us, length us, event | category | flops | bytes accessed | tf_op | source)
XLA Modules:
  0.0 194.7 jit_solution(13674948420204034067)
XLA Ops:
  0.6 187.4 %layer.1 = (bf16[2048,1536]{1,0:T(8,128)(2,1)S(1)}, bf16[2048,1536]{1,0:T(8,128)(2,1)S(1)}, bf16[1536,2048]{1,0:T(8,128)(2,1)S(1)}, bf16[512,512]{1,0:T(8,128)(2,1)S(1)}) custom-call(f32[1,256]{1,0:T(1,128)} %bitcast.1, f32[256,1536]{1,0:T(8,128)} %g_hbm.1, f32[256,1536]{1,0:T(8,128)} %u_hbm.1, f32[768,512]{1,0:T(8,128)} %d_hbm.1, bf16[512,2048]{1,0:T(8,128)(2,1)} %x_hbm.1), custom_call_target="tpu_custom_call" | custom-call | tf_op jit(solution)/shard_map/layer/pallas_call | solution.py:615
  188.0 6.7 %publish.1 = (bf16[2048,1536]{1,0:T(8,128)(2,1)}, bf16[2048,1536]{1,0:T(8,128)(2,1)}, bf16[1536,2048]{1,0:T(8,128)(2,1)}, bf16[512,512]{1,0:T(8,128)(2,1)}) custom-call(bf16[2048,1536]{1,0:T(8,128)(2,1)S(1)} %get-tuple-element.12.wg, bf16[2048,1536]{1,0:T(8,128)(2,1)S(1)} %get-tuple-element.13.wu, bf16[1536,2048]{1,0:T(8,128)(2,1)S(1)} %get-tuple-element.14.wd, ...), custom_call_target="tpu_custom_call" | custom-call | tf_op jit(solution)/shard_map/publish/pallas_call | solution.py:659

commit v4 on v3

--- a/solution.py
+++ b/solution.py
@@ -29,31 +29,13 @@
         pl.loop(lo, hi)(fn)
 
 
-def column_times(pq):
-    tail = 4 * pq - 2 * pq - pq // 2
-    return (
-        [18 + 2 * (p % pq + 1) / pq for p in range(2 * pq)]
-        + [20 + (i + 1) / (pq // 2) for i in range(pq // 2)]
-        + [15 + 6 * (i + 1) / tail for i in range(tail)]
-    )
-
-
-def column_units(pq, nc, paired):
-    times = column_times(pq) if paired else range(nc)
-    if pq % 2:
-        return (), tuple(sorted(range(nc), key=lambda p: times[p]))
-    pairs = sorted(range(0, nc, 2), key=lambda p: max(times[p], times[p + 1]))
-    ends = [p + i for p in pairs[-2:] for i in range(2)]
-    return tuple(pairs[:-2]), tuple(sorted(ends, key=lambda p: (times[p], -p)))
-
-
 def layer_kernel(
     Z, Y, T, nk, paired,
     gain_hbm, g_hbm, u_hbm, d_hbm, x_hbm,
     wg, wu, wd, mixed,
     gain_row, stage_g, stage_u, stage_d, own_d, transit, normed, hidden, part, near, pair, far,
     in_gain, in_g, in_u, in_d, in_x, s_up, s_dn, s_y, s_det, r_w, r_o, s_one, s_tz, s_tx, r_t,
-    s_dz, s_dy, r_d, s_a, r_a, s_b, r_b, r_c,
+    s_dz, s_dy, r_d, s_a, r_a, s_b, r_b,
 ):
     f, t = lax.axis_index("fs"), lax.axis_index("tp")
     X = T // 2
@@ -202,10 +184,6 @@
         fwd_mid = jnp.logical_or(
             jnp.logical_and(can_up, jnp.logical_not(far_up)), jnp.logical_and(can_dn, jnp.logical_not(far_dn))
         )
-        mid_lo, mid_hi = 2 * pq, 2 * pq + pq // 2
-    else:
-        shift = 0
-        mid_lo, mid_hi = 0, nc
     fwd_all = jnp.logical_or(can_up, can_dn)
     if paired:
         passes = jnp.logical_or(fwd_all, beyond)
@@ -214,22 +192,18 @@
     def column(r):
         return lax.rem(r + shift, nc)
 
-    def turned(r):
-        return lax.rem(r + (nc // 2) * (z >= Z // 2).astype(jnp.int32), nc) if paired else r
-
-    def pick(table, i):
-        return turned(sum(p * (i == e).astype(jnp.int32) for e, p in enumerate(table)))
-
-    pair_units, last_units = column_units(pq, nc, paired)
-    sequence = [p + i for p in pair_units for i in range(2)] + list(last_units)
-
-    def piece_of(i):
-        return pick(sequence, i)
-
-    bent = (pq if paired else 0, lambda i: column(core * pq + i))
-    low = (pq if paired else 0, lambda i: column((1 - core) * pq + i))
-    mid = (mid_hi - mid_lo, lambda i: column(mid_lo + i))
-    high = (nc - mid_hi, lambda i: column(mid_hi + i))
+    if paired:
+        bent = (pq, lambda i: column(core * pq + i))
+        low = (pq, lambda i: column((1 - core) * pq + i))
+        mid = (pq // 2, lambda i: column((2 + core) * pq + i))
+        high = (
+            (pq, lambda i: column((3 - core) * pq + i)),
+            (pq // 2, lambda i: column((2 + core) * pq + pq // 2 + i)),
+        )
+    else:
+        mid = (nc, lambda i: i)
+        high = ()
+    high_count = sum(kind[0] for kind in high)
 
     def over(kind, fn):
         each(0, kind[0], lambda i: fn(kind[1](i)))
@@ -239,9 +213,10 @@
 
     def kinds(j):
         r = lax.rem(j - shift + nc, nc)
-        is_high = r >= mid_hi
-        is_bent = both(r < 2 * pq, r // pq == core)
-        return is_high, is_bent, jnp.logical_not(jnp.logical_or(is_high, is_bent))
+        quarter = r // pq
+        is_bent = quarter == core
+        is_mid = jnp.logical_or(quarter == 1 - core, both(quarter == 2 + core, lax.rem(r, pq) < pq // 2))
+        return jnp.logical_not(jnp.logical_or(is_bent, is_mid)), is_bent, is_mid
 
     def z_send(line, j, direction):
         return down(line, j, s_dz.at[direction], (up, dn)[direction])
@@ -263,7 +238,8 @@
             owner = lax.rem(t + i, T)
             for p in range(pq):
                 down_arrived(y, owner * pq + p)
-        over(high, cross)
+        for kind in high:
+            over(kind, cross)
         if paired:
             @pl.when(inner)
             def _():
@@ -298,7 +274,7 @@
 
         @pl.when(here)
         def _():
-            for kind in (low, mid, high):
+            for kind in ((low, mid) if paired else (mid,)) + high:
                 over(kind, lambda j: z_send(y, j, direction).start())
 
     def hook(s):
@@ -341,11 +317,8 @@
         def _():
             @pl.when(jnp.logical_not(inner))
             def _():
-                def late(i):
-                    j = piece_of(i)
-                    is_high, _, _ = kinds(j)
-                    when(jnp.logical_not(is_high), lambda: cross(j))
-                each(0, nc, late)
+                for kind in (bent, low, mid):
+                    over(kind, cross)
             when(inner, lambda: over(bent, cross))
 
     else:
@@ -371,17 +344,19 @@
                     when(near_ok(direction), lambda: z_send(y, j, direction).start())
             over(bent, near_first)
 
-            def near_pair(i):
-                j = piece_of(i)
-                is_high, is_bent, _ = kinds(j)
-
-                @pl.when(jnp.logical_not(is_bent))
-                def _():
+            def near_pair(is_high):
+                def fn(j):
                     near_first(j)
                     down_arrived(other, j)
                     for direction in range(2):
-                        when(jnp.logical_or(near_ok(direction), is_high), lambda: z_send(other, j, direction).start())
-            each(0, nc, near_pair)
+                        toward = can(direction) if is_high else near_ok(direction)
+                        when(toward, lambda: z_send(other, j, direction).start())
+                return fn
+
+            over(low, near_pair(False))
+            for kind in high:
+                over(kind, near_pair(True))
+            over(mid, near_pair(False))
 
     @pl.when(away)
     def _():
@@ -400,12 +375,10 @@
             else:
                 cross(j)
 
-        over(bent, bend)
         if paired:
-            @pl.when(passes)
-            def _():
-                over(low, straight)
-                over(mid, straight)
+            when(passes, lambda: over(low, straight))
+            over(bent, bend)
+            when(passes, lambda: over(mid, straight))
         else:
             over(mid, straight)
 
@@ -430,7 +403,8 @@
                 down_arrived(other, j)
                 for direction in range(2):
                     when(can(direction), lambda: z_send(other, j, direction).start())
-            over(high, twins)
+            for kind in high:
+                over(kind, twins)
 
     for zs in range(Z):
         for o in others:
@@ -468,19 +442,17 @@
     def span(j, count):
         return pl.ds(pl.multiple_of(j * W, W), count * W)
 
-    def height(half, halves):
-        return pl.ds(pl.multiple_of(half * (n // halves), n // halves), n // halves)
-
-    def to_mate(j, count, half, halves, unit):
-        at = (height(half, halves), span(j, count))
-        return copy(part.at[at], near.at[at], s_a.at[0], r_a.at[unit], mate)
-
-    def to_owner(j, count, half, halves, slot, rs, dev):
-        h, p = height(half, halves), lax.rem(j, pq)
-        return copy(pair.at[h, span(j, count)], far.at[slot, h, span(p, count)], s_b.at[0], rs, dev)
-
-    def owner_sem(j, half, halves, slot):
-        return r_b.at[slot, lax.rem(j, pq)] if halves == 1 else r_c.at[slot, lax.rem(j, pq) * halves + half]
+    grain = 2 if pq % 2 == 0 else 1
+
+    def to_mate(j, count):
+        at = span(j, count)
+        return copy(part.at[:, at], near.at[:, at], s_a.at[0], r_a.at[j // grain], mate)
+
+    def to_owner(j, slot, dev):
+        p = lax.rem(j, pq)
+        return copy(
+            pair.at[:, span(j, grain)], far.at[slot, :, span(p, grain)], s_b.at[0], r_b.at[slot, p // grain], dev
+        )
 
     def whole(j):
         if paired:
@@ -497,79 +469,80 @@
     def ours(j):
         return lax.rem(j // pq, 2) == core
 
-    def abroad(j):
-        return both(ours(j), j // pq // 2 != x)
-
-    def products(table, count, halves, lag, base):
-        m = len(table) * halves
-
-        def multiply(j, half):
-            def wait():
-                for i in range(count):
-                    whole(j + i)
-
-            when(half == 0, wait)
-            h, at = height(half, halves), span(j, count)
-            part[h, at] = jnp.dot(hidden[h, :], wd[:, at], preferred_element_type=jnp.float32).astype(jnp.bfloat16)
-
-        def add(j, half, unit):
-            h, at = height(half, halves), span(j, count)
-            when(ours(j), lambda: to_mate(j, count, half, halves, unit).wait_recv())
-
-            @pl.when(abroad(j))
-            def _():
-                pair[h, at] = (part[h, at].astype(jnp.float32) + near[h, at].astype(jnp.float32)).astype(jnp.bfloat16)
-
-        def ship(j, half):
-            owner = j // pq
-            slot = lax.rem(x - owner // 2 + X, X) - 1
-            to_owner(j, count, half, halves, slot, owner_sem(j, half, halves, slot), (f, owner)).start()
-
-        def step(i):
-            now, then = i < m, i >= lag
-            i0, i1 = jnp.minimum(i, m - 1), jnp.maximum(i - lag, 0)
-            j0, j1 = pick(table, i0 // halves), pick(table, i1 // halves)
-            h0, h1 = lax.rem(i0, halves), lax.rem(i1, halves)
-
-            def first_half():
-                when(now, lambda: multiply(j0, h0))
-                when(both(now, jnp.logical_not(ours(j0))), lambda: to_mate(j0, count, h0, halves, base + i).start())
-
-            def second_half():
-                when(then, lambda: add(j1, h1, base + i - lag))
-                when(both(then, abroad(j1)), lambda: ship(j1, h1))
-
-            if lag == 1:
-                second_half()
-                first_half()
-            else:
-                first_half()
-                second_half()
-
-        each(0, m + lag if m else 0, step)
-
-    def finish(table, count, halves):
-        def step(i):
-            j, half = pick(table, i // halves), lax.rem(i, halves)
-
-            @pl.when(j // pq == t)
-            def _():
-                h, at, to = height(half, halves), span(j, count), span(lax.rem(j, pq), count)
-                acc = part[h, at].astype(jnp.float32) + near[h, at].astype(jnp.float32)
-                for slot in range(X - 1):
-                    to_owner(j, count, half, halves, slot, owner_sem(j, half, halves, slot), mate).wait_recv()
-                    acc = acc + far[slot, h, to].astype(jnp.float32)
-                mixed[h, to] = acc.astype(mixed.dtype)
-
-        each(0, len(table) * halves, step)
-
-    early, late_units = last_units[:-2], last_units[-2:]
-    halves = 2 if n % 32 == 0 else 1
-    products(pair_units, 2, 1, 2, 0)
-    products(early, 1, 1, 1, len(pair_units))
-    products(late_units, 1, halves, 2, len(pair_units) + len(early))
-    finish(pair_units, 2, 1)
-    finish(early, 1, 1)
+    def multiply(j, count):
+        for i in range(count):
+            whole(j + i)
+        at = span(j, count)
+        part[:, at] = jnp.dot(hidden[...], wd[:, at], preferred_element_type=jnp.float32).astype(jnp.bfloat16)
+        when(jnp.logical_not(ours(j)), lambda: to_mate(j, count).start())
+
+    def pass_sum(j):
+        owner, at = j // pq, span(j, grain)
+        to_mate(j, grain).wait_recv()
+        pair[:, at] = (part[:, at].astype(jnp.float32) + near[:, at].astype(jnp.float32)).astype(jnp.bfloat16)
+        to_owner(j, lax.rem(x - owner // 2 + X, X) - 1, (f, owner)).start()
+
+    def sums_arrived(j):
+        to_mate(j, grain).wait_recv()
+        for slot in range(X - 1):
+            to_owner(j, slot, mate).wait_recv()
+
+    def finish(j, count):
+        at, to = span(j, count), span(lax.rem(j, pq), count)
+        acc = part[:, at].astype(jnp.float32) + near[:, at].astype(jnp.float32)
+        for slot in range(X - 1):
+            acc = acc + far[slot, :, to].astype(jnp.float32)
+        mixed[:, to] = acc.astype(mixed.dtype)
+
+    if paired:
+        upper = (z >= Z // 2).astype(jnp.int32)
+        is_far = half == 1 - upper
+        is_edge = jnp.logical_or(t == 0, t == T - 1)
+        block_a, block_b, block_c, block_d = core * pq, (1 - core) * pq, (2 + core) * pq, (3 - core) * pq
+        orders = (
+            (block_b, block_d, block_b + 2, block_a, block_d + 2, block_a + 2,
+             block_c + 2, block_c, block_c + 3, block_c + 1),
+            (block_c, block_c + 2, block_b, block_b + 2, block_a + 2, block_d,
+             block_d + 2, block_d + 3, block_a, block_a + 1),
+            (block_c, block_d, block_d + 2, block_c + 2, block_b, block_b + 2,
+             block_a + 2, block_a + 3, block_a, block_a + 1),
+        )
+        turn = upper * (nc // 2)
+        chosen = [
+            lax.rem(jnp.where(is_far, v, jnp.where(is_edge, e, i)) + turn, nc) for v, e, i in zip(*orders)
+        ]
+        doubles, singles = chosen[:6], chosen[6:]
+
+        def pick(table, i):
+            return sum(v * (i == e).astype(jnp.int32) for e, v in enumerate(table))
+
+        over_there = lax.rem(t + T // 2, T) * pq
+        first_at = jnp.where(is_far, 3, jnp.where(is_edge, 0, 5))
+        second_at = jnp.where(is_far, 5, jnp.where(is_edge, 1, 6))
+
+        def double(i):
+            multiply(pick(doubles, i), grain)
+            second = i == second_at
+            when(jnp.logical_or(i == first_at, second), lambda: pass_sum(over_there + second.astype(jnp.int32) * grain))
+
+        def single(i):
+            multiply(pick(singles, i), 1)
+            when(both(i == 0, second_at == 6), lambda: pass_sum(over_there + grain))
+
+        each(0, len(doubles), double)
+        each(0, len(singles) - 1, single)
+        each(0, pq // grain, lambda i: sums_arrived(t * pq + i * grain))
+        finish(t * pq + 2, 2)
+        finish(t * pq, 1)
+        multiply(singles[-1], 1)
+        finish(t * pq + 1, 1)
+    else:
+        each(0, nc // grain, lambda i: multiply(i * grain, grain))
+        for i in range(1, X):
+            base = (lax.rem(x + i, X) * 2 + core) * pq
+            each(0, pq // grain, lambda i, base=base: pass_sum(base + i * grain))
+        each(0, pq // grain, lambda i: sums_arrived(t * pq + i * grain))
+        each(0, pq // grain, lambda i: finish(t * pq + i * grain, grain))
 
     def gone(sem, ref):
         copy(ref, ref, sem, r_a.at[0], mate).wait_send()
@@ -585,16 +558,15 @@
         for direction in range(2):
             gone_down(both(can(direction), near_ok(direction)), s_dz.at[direction], 2 * nc - pq)
             on = both(can(direction), jnp.logical_not(near_ok(direction)))
-            gone_down(on, s_dz.at[direction], nc - pq + high[0])
+            gone_down(on, s_dz.at[direction], nc - pq + high_count)
         gone_down(at_home, s_dy.at[0], nc)
-        gone_down(beyond, s_dy.at[0], nc - high[0])
+        gone_down(beyond, s_dy.at[0], nc - high_count)
         gone_down(both(away, jnp.logical_not(beyond)), s_dy.at[0], pq)
     else:
         for direction in range(2):
             gone_down(can(direction), s_dz.at[direction], nc)
         for i in range(Y - 1):
             gone_down(z >= 0, s_dy.at[i], nc)
-    finish(late_units, 1, halves)
     gone(s_a.at[0], part.at[:, pl.ds(0, nc * W // 2)])
     gone(s_b.at[0], pair.at[:, pl.ds(0, (X - 1) * pq * W)])
 
@@ -607,7 +579,8 @@
     pq = d.shape[1] // W
     nc = T * pq
     nk = max(1, min(4, rows // 64))
-    paired = Y == 2 and X == 2 and Z == T and pq % 2 == 0
+    paired = Y == 2 and X == 2 and Z == T and pq == 4
+    grain = 2 if pq % 2 == 0 else 1
     lanes = max(Y - 1, 1)
     dma = pltpu.SemaphoreType.DMA
     vmem, hbm = pl.BlockSpec(memory_space=pltpu.VMEM), pl.BlockSpec(memory_space=pltpu.HBM)
@@ -632,8 +605,7 @@
             dma((1,)), dma((1,)), dma((lanes,)), dma((1,)), dma((Z, nk)), dma((fs,)),
             dma((1,)), dma((1,)), dma((1,)), dma((pq,)),
             dma((2,)), dma((lanes,)), dma((Y, nc)),
-            dma((1,)), dma((sum(map(len, column_units(pq, nc, paired))) + 2,)), dma((1,)), dma((max(X - 1, 1), pq)),
-            dma((max(X - 1, 1), 2 * pq)),
+            dma((1,)), dma((nc // grain,)), dma((1,)), dma((max(X - 1, 1), pq // grain)),
         ],
         compiler_params=pltpu.CompilerParams(
             collective_id=0, has_side_effects=True, vmem_limit_bytes=GRANT

time: 195 us -> 193 us (0.990)
  Pallas kernels: 194 us -> 191 us
    pallas_call x1, Pallas kernels: 187 us -> 184 us  [layer(): pl.pallas_call(functools.partial(layer_kernel, Z, Y, T, nk, paired), out_...]
where the time goes in v4:
time: 193 us; the launch traced here: 191 us
  Pallas kernels  191 us (99%)
    pallas_call x1, Pallas kernels, layer(): pl.pallas_call(functools.partial(layer_kernel, Z, Y, T, nk, paired), out_...  184 us
    pallas_call x1, Pallas kernels, publish(): pl.pallas_call(functools.partial(publish_kernel, CUTS), out_shape=tuple((...  6.73 us

profile of v4, /device:TPU:0, one launch (start us, length us, event | category | flops | bytes accessed | tf_op | source)
XLA Modules:
  0.0 191.4 jit_solution(16863197914290369055)
XLA Ops:
  0.6 184.1 %layer.1 = (bf16[2048,1536]{1,0:T(8,128)(2,1)S(1)}, bf16[2048,1536]{1,0:T(8,128)(2,1)S(1)}, bf16[1536,2048]{1,0:T(8,128)(2,1)S(1)}, bf16[512,512]{1,0:T(8,128)(2,1)S(1)}) custom-call(f32[1,256]{1,0:T(1,128)} %bitcast.1, f32[256,1536]{1,0:T(8,128)} %g_hbm.1, f32[256,1536]{1,0:T(8,128)} %u_hbm.1, f32[768,512]{1,0:T(8,128)} %d_hbm.1, bf16[512,2048]{1,0:T(8,128)(2,1)} %x_hbm.1), custom_call_target="tpu_custom_call" | custom-call | tf_op jit(solution)/shard_map/layer/pallas_call | solution.py:588
  184.7 6.7 %publish.1 = (bf16[2048,1536]{1,0:T(8,128)(2,1)}, bf16[2048,1536]{1,0:T(8,128)(2,1)}, bf16[1536,2048]{1,0:T(8,128)(2,1)}, bf16[512,512]{1,0:T(8,128)(2,1)}) custom-call(bf16[2048,1536]{1,0:T(8,128)(2,1)S(1)} %get-tuple-element.12.wg, bf16[2048,1536]{1,0:T(8,128)(2,1)S(1)} %get-tuple-element.13.wu, bf16[1536,2048]{1,0:T(8,128)(2,1)S(1)} %get-tuple-element.14.wd, ...), custom_call_target="tpu_custom_call" | custom-call | tf_op jit(solution)/shard_map/publish/pallas_call | solution.py:631

commit v5 on v4

--- a/solution.py
+++ b/solution.py
@@ -445,13 +445,16 @@
     grain = 2 if pq % 2 == 0 else 1
 
     def to_mate(j, count):
-        at = span(j, count)
-        return copy(part.at[:, at], near.at[:, at], s_a.at[0], r_a.at[j // grain], mate)
-
-    def to_owner(j, slot, dev):
+        at, lone = span(j, count), j // grain
+        if count < grain:
+            odd = lax.rem(j, grain)
+            lone = odd * (nc // grain) + (1 - odd) * lone
+        return copy(part.at[:, at], near.at[:, at], s_a.at[0], r_a.at[lone], mate)
+
+    def to_owner(j, count, slot, dev):
         p = lax.rem(j, pq)
         return copy(
-            pair.at[:, span(j, grain)], far.at[slot, :, span(p, grain)], s_b.at[0], r_b.at[slot, p // grain], dev
+            pair.at[:, span(j, count)], far.at[slot, :, span(p, count)], s_b.at[0], r_b.at[slot, p // grain], dev
         )
 
     def whole(j):
@@ -476,16 +479,16 @@
         part[:, at] = jnp.dot(hidden[...], wd[:, at], preferred_element_type=jnp.float32).astype(jnp.bfloat16)
         when(jnp.logical_not(ours(j)), lambda: to_mate(j, count).start())
 
-    def pass_sum(j):
-        owner, at = j // pq, span(j, grain)
-        to_mate(j, grain).wait_recv()
+    def pass_sum(j, count):
+        owner, at = j // pq, span(j, count)
+        to_mate(j, count).wait_recv()
         pair[:, at] = (part[:, at].astype(jnp.float32) + near[:, at].astype(jnp.float32)).astype(jnp.bfloat16)
-        to_owner(j, lax.rem(x - owner // 2 + X, X) - 1, (f, owner)).start()
+        to_owner(j, count, lax.rem(x - owner // 2 + X, X) - 1, (f, owner)).start()
 
     def sums_arrived(j):
         to_mate(j, grain).wait_recv()
         for slot in range(X - 1):
-            to_owner(j, slot, mate).wait_recv()
+            to_owner(j, grain, slot, mate).wait_recv()
 
     def finish(j, count):
         at, to = span(j, count), span(lax.rem(j, pq), count)
@@ -523,11 +526,11 @@
         def double(i):
             multiply(pick(doubles, i), grain)
             second = i == second_at
-            when(jnp.logical_or(i == first_at, second), lambda: pass_sum(over_there + second.astype(jnp.int32) * grain))
+            when(jnp.logical_or(i == first_at, second), lambda: pass_sum(over_there + second.astype(jnp.int32) * grain, grain))
 
         def single(i):
             multiply(pick(singles, i), 1)
-            when(both(i == 0, second_at == 6), lambda: pass_sum(over_there + grain))
+            when(both(i < grain, second_at == 6), lambda: pass_sum(over_there + grain + i, 1))
 
         each(0, len(doubles), double)
         each(0, len(singles) - 1, single)
@@ -540,7 +543,7 @@
         each(0, nc // grain, lambda i: multiply(i * grain, grain))
         for i in range(1, X):
             base = (lax.rem(x + i, X) * 2 + core) * pq
-            each(0, pq // grain, lambda i, base=base: pass_sum(base + i * grain))
+            each(0, pq // grain, lambda i, base=base: pass_sum(base + i * grain, grain))
         each(0, pq // grain, lambda i: sums_arrived(t * pq + i * grain))
         each(0, pq // grain, lambda i: finish(t * pq + i * grain, grain))
 
@@ -605,7 +608,7 @@
             dma((1,)), dma((1,)), dma((lanes,)), dma((1,)), dma((Z, nk)), dma((fs,)),
             dma((1,)), dma((1,)), dma((1,)), dma((pq,)),
             dma((2,)), dma((lanes,)), dma((Y, nc)),
-            dma((1,)), dma((nc // grain,)), dma((1,)), dma((max(X - 1, 1), pq // grain)),
+            dma((1,)), dma((nc // grain + 1,)), dma((1,)), dma((max(X - 1, 1), pq // grain)),
         ],
         compiler_params=pltpu.CompilerParams(
             collective_id=0, has_side_effects=True, vmem_limit_bytes=GRANT

time: 193 us -> 192 us (level)
  no operation moved by 1% of the time
where the time goes in v5:
time: 192 us; the launch traced here: 191 us
  Pallas kernels  191 us (99%)
    pallas_call x1, Pallas kernels, layer(): pl.pallas_call(functools.partial(layer_kernel, Z, Y, T, nk, paired), out_...  184 us
    pallas_call x1, Pallas kernels, publish(): pl.pallas_call(functools.partial(publish_kernel, CUTS), out_shape=tuple((...  6.73 us

profile of v5, /device:TPU:0, one launch (start us, length us, event | category | flops | bytes accessed | tf_op | source)
XLA Modules:
  0.0 191.4 jit_solution(9886778687421999861)
XLA Ops:
  0.6 184.1 %layer.1 = (bf16[2048,1536]{1,0:T(8,128)(2,1)S(1)}, bf16[2048,1536]{1,0:T(8,128)(2,1)S(1)}, bf16[1536,2048]{1,0:T(8,128)(2,1)S(1)}, bf16[512,512]{1,0:T(8,128)(2,1)S(1)}) custom-call(f32[1,256]{1,0:T(1,128)} %bitcast.1, f32[256,1536]{1,0:T(8,128)} %g_hbm.1, f32[256,1536]{1,0:T(8,128)} %u_hbm.1, f32[768,512]{1,0:T(8,128)} %d_hbm.1, bf16[512,2048]{1,0:T(8,128)(2,1)} %x_hbm.1), custom_call_target="tpu_custom_call" | custom-call | tf_op jit(solution)/shard_map/layer/pallas_call | solution.py:591
  184.7 6.7 %publish.1 = (bf16[2048,1536]{1,0:T(8,128)(2,1)}, bf16[2048,1536]{1,0:T(8,128)(2,1)}, bf16[1536,2048]{1,0:T(8,128)(2,1)}, bf16[512,512]{1,0:T(8,128)(2,1)}) custom-call(bf16[2048,1536]{1,0:T(8,128)(2,1)S(1)} %get-tuple-element.12.wg, bf16[2048,1536]{1,0:T(8,128)(2,1)S(1)} %get-tuple-element.13.wu, bf16[1536,2048]{1,0:T(8,128)(2,1)S(1)} %get-tuple-element.14.wd, ...), custom_call_target="tpu_custom_call" | custom-call | tf_op jit(solution)/shard_map/publish/pallas_call | solution.py:634

commit v6 on v5

--- a/solution.py
+++ b/solution.py
@@ -533,11 +533,11 @@
             when(both(i < grain, second_at == 6), lambda: pass_sum(over_there + grain + i, 1))
 
         each(0, len(doubles), double)
-        each(0, len(singles) - 1, single)
+        each(0, len(singles), lambda i: when(jnp.logical_or(i < len(singles) - 1, is_far), lambda: single(i)))
         each(0, pq // grain, lambda i: sums_arrived(t * pq + i * grain))
         finish(t * pq + 2, 2)
         finish(t * pq, 1)
-        multiply(singles[-1], 1)
+        when(jnp.logical_not(is_far), lambda: multiply(singles[-1], 1))
         finish(t * pq + 1, 1)
     else:
         each(0, nc // grain, lambda i: multiply(i * grain, grain))

time: 192 us -> 192 us (level)
  no operation moved by 1% of the time
where the time goes in v6:
time: 192 us; the launch traced here: 191 us
  Pallas kernels  191 us (99%)
    pallas_call x1, Pallas kernels, layer(): pl.pallas_call(functools.partial(layer_kernel, Z, Y, T, nk, paired), out_...  184 us
    pallas_call x1, Pallas kernels, publish(): pl.pallas_call(functools.partial(publish_kernel, CUTS), out_shape=tuple((...  6.73 us

profile of v6, /device:TPU:0, one launch (start us, length us, event | category | flops | bytes accessed | tf_op | source)
XLA Modules:
  0.0 191.4 jit_solution(8124661174824297385)
XLA Ops:
  0.6 184.1 %layer.1 = (bf16[2048,1536]{1,0:T(8,128)(2,1)S(1)}, bf16[2048,1536]{1,0:T(8,128)(2,1)S(1)}, bf16[1536,2048]{1,0:T(8,128)(2,1)S(1)}, bf16[512,512]{1,0:T(8,128)(2,1)S(1)}) custom-call(f32[1,256]{1,0:T(1,128)} %bitcast.1, f32[256,1536]{1,0:T(8,128)} %g_hbm.1, f32[256,1536]{1,0:T(8,128)} %u_hbm.1, f32[768,512]{1,0:T(8,128)} %d_hbm.1, bf16[512,2048]{1,0:T(8,128)(2,1)} %x_hbm.1), custom_call_target="tpu_custom_call" | custom-call | tf_op jit(solution)/shard_map/layer/pallas_call | solution.py:591
  184.7 6.7 %publish.1 = (bf16[2048,1536]{1,0:T(8,128)(2,1)}, bf16[2048,1536]{1,0:T(8,128)(2,1)}, bf16[1536,2048]{1,0:T(8,128)(2,1)}, bf16[512,512]{1,0:T(8,128)(2,1)}) custom-call(bf16[2048,1536]{1,0:T(8,128)(2,1)S(1)} %get-tuple-element.12.wg, bf16[2048,1536]{1,0:T(8,128)(2,1)S(1)} %get-tuple-element.13.wu, bf16[1536,2048]{1,0:T(8,128)(2,1)S(1)} %get-tuple-element.14.wd, ...), custom_call_target="tpu_custom_call" | custom-call | tf_op jit(solution)/shard_map/publish/pallas_call | solution.py:634
